TPU v7x, 256 devices: a 4x2x16 block of a 4x16x16 slice. The times are simulated.
256 devices in a mesh: grp: 2 (over y), ep: 64 (over z, x), tp: 2 (over core).
Axes of the slice: x: 4, y: 2, z: 16, core: 2. Of those that a mesh axis runs over, the one named last changes fastest.
The devices are a block of a 4x16x16 slice.
Arguments:
- tokens: bfloat16 [12288, 2048], P(('grp', 'ep')), parts along dimension 0, may hold values from -6 to 6
- prior_state: float32 [2, 12288, 4096], P(None, ('grp', 'ep'), 'tp'), parts along dimension 1, may hold values from -6 to 6
- mix_gain: float32 [2048], replicated, may hold values from 0.1 to 1.9
- in_weight: bfloat16 [2048, 1024], P(None, 'tp'), may hold values from -0.125 to 0.125
- decay_rate: float32 [64, 64], P('tp'), may hold values from 0.2 to 20
- frequency: float32 [64, 64], P('tp'), may hold values from 0 to 12
- log_step: float32 [64], P('tp'), may hold values from -4.6 to 0
- input_map: float32 [2, 64, 64, 16], P(None, 'tp'), may hold values from -6 to 6
- output_map: float32 [2, 64, 16, 64], P(None, 'tp'), may hold values from -0.5 to 0.5
- skip_gain: float32 [1024], P('tp'), may hold values from -4 to 4
- out_weight: bfloat16 [1024, 2048], P('tp'), may hold values from -0.1875 to 0.1875
- channel_gain: float32 [2048], replicated, may hold values from 0.1 to 1.9
- expert_gate: bfloat16 [64, 2048, 512], P('ep', None, 'tp'), may hold values from -0.125 to 0.125
- expert_up: bfloat16 [64, 2048, 512], P('ep', None, 'tp'), may hold values from -0.125 to 0.125
- expert_down: bfloat16 [64, 512, 2048], P('ep', 'tp'), may hold values from -0.25 to 0.25
- shared_gate: bfloat16 [2048, 512], P(None, 'tp'), may hold values from -0.125 to 0.125
- shared_up: bfloat16 [2048, 512], P(None, 'tp'), may hold values from -0.125 to 0.125
- shared_down: bfloat16 [512, 2048], P('tp'), may hold values from -0.25 to 0.25
- routes: int32 [12288, 6], P(('grp', 'ep')), parts along dimension 0, may hold values from 0 to 63, all different within a row; in each aligned block of 96 rows (0 to 95, 96 to 191, ...) at most 13 rows name the same one
- route_weights: float32 [12288, 6], P(('grp', 'ep')), parts along dimension 0, may hold values from 0.05 to 0.8
Outputs:
- layer_out: bfloat16 [12288, 2048], P(('grp', 'ep'), 'tp'), parts along dimension 0
- new_state: float32 [2, 12288, 4096], P(None, ('grp', 'ep'), 'tp'), parts along dimension 1
There are 2 independent parts, one for each index of `grp`. A program takes and returns all parts, laid end to end along the dimension named above; an argument that names none is the same for every part. Nothing has to cross between parts.
Inputs may be any that keep to these rules, and one draw needn't show every extreme that they name: `routes`: each row names 6 different experts; among the rows of one index of ep no expert is named by more than 13 rows.
All inputs are finite; a program needn't handle non-finite values.
Results may differ from a plain program's by a relative error of at most 0.017.
Values may be sent and summed in bfloat16 or wider, within the bound.
No kernel may reach another device: no remote copies, remote signals or barrier semaphores. Data moves between devices by JAX's collectives and lax.ppermute only.
A program may use at most 128 MiB of HBM per device.

v0:
```python
import functools

import jax
import jax.numpy as jnp
from jax import lax
from jax.experimental import pallas as pl
from jax.experimental.pallas import tpu as pltpu
from jax.sharding import PartitionSpec as P

norm_eps = 1e-06
RING = 4
NEAR = 4
TABLE, TOP, LANES = 8, 6, 128
AXES = ("ep", "tp")
f32, bf16 = jnp.float32, jnp.bfloat16
BIG = pltpu.CompilerParams(vmem_limit_bytes=24 * 1024 * 1024)
VM = pl.BlockSpec(memory_space=pltpu.VMEM)
SM = pl.BlockSpec(memory_space=pltpu.SMEM)


def held(value):
    return pltpu.with_memory_space_constraint(value, pltpu.VMEM)


def dot(a, b):
    return jnp.dot(a, b, preferred_element_type=f32)


def scaled(values, gain):
    factor = lax.rsqrt(jnp.mean(values * values, axis=-1, keepdims=True) + norm_eps)
    return (values * factor * gain).astype(bf16)


def turn_and_hold(decay_rate, frequency, log_step):
    step_size = jnp.exp(log_step)
    real_rate = -decay_rate
    magnitude = jnp.exp(real_rate * step_size)
    turn_real = magnitude * jnp.cos(frequency * step_size)
    turn_imag = magnitude * jnp.sin(frequency * step_size)
    denominator = real_rate * real_rate + frequency * frequency
    hold_real = ((turn_real - 1.0) * real_rate + turn_imag * frequency) / denominator
    hold_imag = (turn_imag * real_rate - (turn_real - 1.0) * frequency) / denominator
    return turn_real, turn_imag, hold_real, hold_imag


def mixer_kernel(
    tok, gain, w_in, state, decay, freq, log_step, imap, omap, skip, w_out, fresh, partial, normed, acc
):
    step = pl.program_id(0)

    @pl.when(step == 0)
    def _():
        normed[...] = scaled(tok[...].astype(f32), gain[...])

    drive = dot(normed[...], w_in[...]).astype(bf16)
    chans, entries = imap.shape[1], imap.shape[2]
    groups = decay.shape[0]
    width, wide = chans // groups, groups * entries
    same = (lax.broadcasted_iota(jnp.int32, (chans, wide), 0) // width) == (
        lax.broadcasted_iota(jnp.int32, (chans, wide), 1) // entries
    )

    def spread(m):
        return jnp.where(same, jnp.concatenate([m] * groups, axis=1), 0.0).astype(bf16)

    def row(m):
        return jnp.concatenate([m[g : g + 1, :] for g in range(groups)], axis=1)

    push_re, push_im = dot(drive, spread(imap[0])), dot(drive, spread(imap[1]))
    spread_out = (groups, log_step.shape[1])
    wanted = step * groups + lax.broadcasted_iota(jnp.int32, spread_out, 0)
    chosen = wanted == lax.broadcasted_iota(jnp.int32, spread_out, 1)
    log_steps = jnp.sum(jnp.where(chosen, log_step[...], 0.0), axis=1, keepdims=True)
    coef = turn_and_hold(decay[...], freq[...], log_steps)
    turn_re, turn_im, hold_re, hold_im = [row(c) for c in coef]
    old_re, old_im = state[0], state[1]
    new_re = turn_re * old_re - turn_im * old_im + (push_re * hold_re - push_im * hold_im)
    new_im = turn_re * old_im + turn_im * old_re + (push_re * hold_im + push_im * hold_re)
    fresh[0] = new_re
    fresh[1] = new_im
    nt = (((1,), (1,)), ((), ()))
    readout = lax.dot_general(
        new_re.astype(bf16), spread(omap[0]), nt, preferred_element_type=f32
    ) - lax.dot_general(new_im.astype(bf16), spread(omap[1]), nt, preferred_element_type=f32)
    readout = readout + skip[...] * drive.astype(f32)
    part = dot(jax.nn.gelu(readout).astype(bf16), w_out[...])

    @pl.when(step == 0)
    def _():
        acc[...] = part

    @pl.when(step > 0)
    def _():
        acc[...] += part

    @pl.when(step == pl.num_programs(0) - 1)
    def _():
        partial[...] = acc[...].astype(bf16)


def mixer(tokens, gain, w_in, state, decay, freq, log_step, imap, omap, skip, w_out):
    rows, width = tokens.shape
    chans = w_in.shape[1]
    groups, entries = decay.shape
    steps = 4
    c, g, s = chans // steps, groups // steps, groups * entries // steps
    return pl.pallas_call(
        mixer_kernel,
        grid=(steps,),
        in_specs=[
            VM,
            pl.BlockSpec((1, width), lambda i: (0, 0)),
            pl.BlockSpec((width, c), lambda i: (0, i)),
            pl.BlockSpec((2, rows, s), lambda i: (0, 0, i)),
            pl.BlockSpec((g, entries), lambda i: (i, 0)),
            pl.BlockSpec((g, entries), lambda i: (i, 0)),
            pl.BlockSpec((1, groups), lambda i: (0, 0)),
            pl.BlockSpec((2, c, entries), lambda i: (0, i, 0)),
            pl.BlockSpec((2, c, entries), lambda i: (0, i, 0)),
            pl.BlockSpec((1, c), lambda i: (0, i)),
            pl.BlockSpec((c, width), lambda i: (i, 0)),
        ],
        out_specs=[pl.BlockSpec((2, rows, s), lambda i: (0, 0, i)), VM],
        out_shape=[jax.ShapeDtypeStruct(state.shape, f32), pltpu.VMEM((rows, width), bf16)],
        scratch_shapes=[pltpu.VMEM((rows, width), bf16), pltpu.VMEM((rows, width), f32)],
        compiler_params=pltpu.CompilerParams(vmem_limit_bytes=56 * 1024 * 1024),
        name="mixer",
    )(tokens, gain, w_in, state, decay, freq, log_step, imap, omap, skip, w_out)


def call(kernel, scalar, arrays, outs, scratch=()):
    return pl.pallas_call(
        kernel,
        in_specs=[SM] + [VM] * len(arrays),
        out_specs=[VM] * len(outs),
        out_shape=[pltpu.VMEM(shape, dtype) for shape, dtype in outs],
        scratch_shapes=list(scratch),
        compiler_params=BIG,
    )(scalar, *[held(a) for a in arrays])


def second_norm_kernel(
    spot, tok, mine, other, gain, table, own_half, far_half, mid_half, left, right, normed, mid
):
    core = spot[0] % 2
    rows, half = far_half.shape
    middle = (tok[...].astype(f32) + (mine[...].astype(f32) + other[...].astype(f32))).astype(bf16)
    mid[...] = middle
    normed[...] = scaled(middle.astype(f32), gain[...])
    here = pl.multiple_of(core * half, half)
    there = pl.multiple_of((1 - core) * half, half)
    own = normed[:, pl.ds(here, half)]
    own_half[...] = own
    left[:rows, :] = own[:, : half // 2]
    left[rows:, :] = table[...]
    right[...] = own[:, half // 2 :]
    far_half[...] = normed[:, pl.ds(there, half)]
    mid_half[...] = mid[:, pl.ds(here, half)]


def second_norm(spot, tokens, mine, other, gain, table):
    rows, width = tokens.shape
    half = width // 2
    return call(
        second_norm_kernel,
        spot,
        (tokens, mine, other, gain, table),
        [((rows, half), bf16)] * 3
        + [((rows + TABLE, half // 2), bf16), ((rows, half // 2), bf16)],
        [pltpu.VMEM((rows, width), bf16), pltpu.VMEM((rows, width), bf16)],
    )


def block_kernel(first, spot, own, other, gate, up, down, keep, send):
    core = spot[0] % 2
    rows, half = other.shape
    here = pl.multiple_of(core * half, half)
    there = pl.multiple_of((1 - core) * half, half)
    tile = rows // -(-rows // 256)
    for i in range(0, rows, tile):
        a, b = own[first + i : first + i + tile, :], other[i : i + tile, :]
        gate_val = dot(a, gate[pl.ds(here, half), :]) + dot(b, gate[pl.ds(there, half), :])
        up_val = dot(a, up[pl.ds(here, half), :]) + dot(b, up[pl.ds(there, half), :])
        hidden = (jax.nn.silu(gate_val) * up_val).astype(bf16)
        send[i : i + tile, :] = dot(hidden, down[:, pl.ds(there, half)]).astype(bf16)
        keep[i : i + tile, :] = dot(hidden, down[:, pl.ds(here, half)]).astype(bf16)


def block(spot, own, other, gate, up, down, first):
    return call(
        functools.partial(block_kernel, first),
        spot,
        (own, other, gate, up, down),
        [(other.shape, bf16)] * 2,
    )


def slots_of(spot, cap, planes, slots, m, table, pick, mix):
    core, plane = spot[0] % 2, spot[0] // (2 * RING)
    base = plane + 2 * core
    base = jnp.where(base >= planes, base - planes, base) // NEAR * NEAR
    dests, rows = NEAR * RING, pick.shape[1]
    order = lax.broadcasted_iota(jnp.int32, (dests, 1), 0)
    near, across = order // RING, order % RING
    at = base + near - jnp.where(near >= NEAR // 2, NEAR * core, 0)
    at = jnp.where(at < 0, at + planes, at)
    expert = (at * RING + across).astype(f32)
    before = lax.broadcasted_iota(jnp.int32, (rows, rows), 0) < lax.broadcasted_iota(
        jnp.int32, (rows, rows), 1
    )
    before = before.astype(f32).astype(bf16)
    level = lax.broadcasted_iota(jnp.int32, (slots, rows), 0).astype(f32)
    hits = jnp.zeros((dests, rows), f32)
    weight = jnp.zeros((dests, rows), f32)
    for k in range(TOP):
        hit = (table[k : k + 1, :rows] == expert).astype(f32)
        hits = hits + hit
        weight = weight + hit * table[k : k + 1, LANES : LANES + rows]
    rank = dot(hits.astype(bf16), before)
    home = plane - NEAR * m
    home = jnp.where(home < 0, home + planes, home) // NEAR
    place = jnp.where(hits > 0.5, rank + (home * cap).astype(f32), -1.0)
    for d in range(0, dests, 2):
        ones = [(level == place[e : e + 1, :]).astype(f32) for e in (d, d + 1)]
        mixed = [one * weight[e : e + 1, :] for one, e in zip(ones, (d, d + 1))]
        span = pl.ds(d * slots, 2 * slots)
        pick[span, :] = jnp.concatenate(ones, axis=0).astype(bf16)
        mix[span, :] = jnp.concatenate(mixed, axis=0).astype(bf16)


def table_of(ref, rows):
    return ref[rows:, : 2 * LANES].astype(f32)


def relay_near_kernel(
    cap, planes, slots, spot, own_l, own_r, below_l, below_r, above_l, above_r, part, mix, pick
):
    rows = pick.shape[2]
    half = own_r.shape[1]
    for i, (m, ref) in enumerate(((0, own_l), (1, below_l), (3, above_l))):
        slots_of(spot, cap, planes, slots, m, table_of(ref, rows), pick.at[i], mix.at[i])
    tile = 2 * slots
    for i in range(0, part.shape[0], tile):
        span = pl.ds(i, tile)
        for at, refs in (
            (slice(0, half), (own_l, below_l, above_l)),
            (slice(half, None), (own_r, below_r, above_r)),
        ):
            sums = [dot(pick[n, span, :], ref[:rows, :]) for n, ref in enumerate(refs)]
            part[span, at] = (sums[0] + sums[1] + sums[2]).astype(bf16)


def relay_far_kernel(cap, planes, slots, spot, far_l, far_r, part, out, mix, pick):
    rows = pick.shape[1]
    half = far_r.shape[1]
    slots_of(spot, cap, planes, slots, 2, table_of(far_l, rows), pick, mix)
    tile = 2 * slots
    for i in range(0, part.shape[0], tile):
        span = pl.ds(i, tile)
        one = pick[span, :]
        out[span, :half] = part[span, :half] + dot(one, far_l[:rows, :]).astype(bf16)
        out[span, half:] = part[span, half:] + dot(one, far_r[...]).astype(bf16)


TN = (((0,), (0,)), ((), ()))


def mix_far_kernel(spot, mix, back, left, right):
    half = left.shape[1]
    far = lax.dot_general(mix[...], back[...], TN, preferred_element_type=f32).astype(bf16)
    left[...] = far[:, :half]
    right[...] = far[:, half:]


def mix_near_kernel(spot, mix, back, own, below_l, below_r, above_l, above_r):
    half = below_l.shape[1]
    for i, (left, right) in ((1, (below_l, below_r)), (2, (above_l, above_r))):
        sums = lax.dot_general(mix[i], back[...], TN, preferred_element_type=f32)
        left[...] = sums[:, :half].astype(left.dtype)
        right[...] = sums[:, half:].astype(right.dtype)
    own[...] = lax.dot_general(mix[0], back[...], TN, preferred_element_type=f32)


def body(
    tokens,
    prior_state,
    mix_gain,
    in_weight,
    decay_rate,
    frequency,
    log_step,
    input_map,
    output_map,
    skip_gain,
    out_weight,
    channel_gain,
    expert_gate,
    expert_up,
    expert_down,
    shared_gate,
    shared_up,
    shared_down,
    routes,
    route_weights,
):
    experts, cores = lax.axis_size("ep"), lax.axis_size("tp")
    planes = experts // RING
    spot = lax.axis_index(AXES).astype(jnp.int32).reshape(1)
    seq_rows, top_count = routes.shape
    slot_cap = min(seq_rows, max(2, 3 * seq_rows * top_count // (2 * experts)))
    slots = -(-4 * slot_cap // 8) * 8
    total = NEAR * RING * slots
    width = tokens.shape[1]
    wide = width // 2
    half = wide // 2

    def at(z, x, t):
        return ((z % planes) * RING + x) * cores + t

    everyone = [(z, x, t) for z in range(planes) for x in range(RING) for t in range(cores)]

    def along(value, offset):
        return lax.ppermute(
            value, AXES, [(at(z, x, t), at(z + offset, x, t)) for z, x, t in everyone]
        )

    def swap(value):
        return lax.ppermute(value, "tp", [(t, cores - 1 - t) for t in range(cores)])

    nearby = [
        [
            at(NEAR * (q - (t if j >= NEAR // 2 else 0)) + j, x, t)
            for j in range(NEAR)
            for x in range(RING)
        ]
        for q in range(planes // NEAR)
        for t in range(cores)
    ]

    def exchange(value):
        tiles = value.reshape(NEAR * RING, slots, value.shape[1])
        tiles = lax.all_to_all(tiles, AXES, 0, 0, axis_index_groups=nearby, tiled=True)
        return tiles.reshape(value.shape)

    table = jnp.concatenate(
        [
            jnp.pad(value.T.astype(bf16), ((0, TABLE - top_count), (0, LANES - seq_rows)))
            for value in (routes, route_weights)
        ],
        axis=1,
    )
    table = jnp.pad(table, ((0, 0), (0, half - 2 * LANES)))

    lanes = input_map.shape[2]
    imap = input_map.transpose(0, 1, 3, 2).reshape(2, -1, lanes)
    omap = output_map.reshape(2, -1, lanes)
    new_state, partial = mixer(
        tokens,
        mix_gain[None],
        in_weight,
        prior_state,
        decay_rate,
        frequency,
        log_step[None],
        imap,
        omap,
        skip_gain[None],
        out_weight,
    )
    own, other, middle, own_l, own_r = second_norm(
        spot, tokens, partial, swap(partial), channel_gain[None], table
    )

    below_l, above_r = along(own_l, NEAR), along(own_r, -NEAR)
    below_r, above_l = along(own_r, NEAR), along(own_l, -NEAR)
    far_l, far_r = along(below_l, NEAR), along(above_r, -NEAR)
    shared_keep, shared_send = block(spot, own, other, shared_gate, shared_up, shared_down, 0)
    shared_recv = swap(shared_send)
    sizes = (slot_cap, planes, slots)
    part, mix_near = call(
        functools.partial(relay_near_kernel, *sizes),
        spot,
        (own_l, own_r, below_l, below_r, above_l, above_r),
        [((total, wide), bf16), ((3, total, seq_rows), bf16)],
        [pltpu.VMEM((3, total, seq_rows), bf16)],
    )
    part, shared_keep, shared_recv = lax.optimization_barrier((part, shared_keep, shared_recv))
    rows, mix_far = call(
        functools.partial(relay_far_kernel, *sizes),
        spot,
        (far_l, far_r, part),
        [((total, wide), bf16), ((total, seq_rows), bf16)],
        [pltpu.VMEM((total, seq_rows), bf16)],
    )

    arrived = exchange(rows)
    cut = total // 2
    others = [swap(arrived[i : i + cut]) for i in (0, cut)]
    weights = (expert_gate[0], expert_up[0], expert_down[0])
    outs = [block(spot, arrived, o, *weights, i) for o, i in zip(others, (0, cut))]
    summed = [keep.astype(f32) + swap(send).astype(f32) for keep, send in outs]
    back = exchange(jnp.concatenate(summed, axis=0).astype(bf16))

    sent, sums = ((seq_rows, half), bf16), ((seq_rows, half), f32)
    m_far_l, m_far_r = call(mix_far_kernel, spot, (mix_far, back), [sent] * 2)
    in_l, in_r = along(m_far_l, NEAR), along(m_far_r, -NEAR)
    m_own, m_below_l, m_below_r, m_above_l, m_above_r = call(
        mix_near_kernel, spot, (mix_near, back), [((seq_rows, wide), f32), sent, sums, sums, sent]
    )
    below_right, above_left = along(m_above_r, NEAR), along(m_below_l, -NEAR)
    below_left = along((m_above_l + in_l.astype(f32)).astype(bf16), NEAR)
    above_right = along((m_below_r + in_r.astype(f32)).astype(bf16), -NEAR)
    shared_out = shared_keep.astype(f32) + shared_recv.astype(f32)
    rest = middle.astype(f32) + shared_out + m_own
    left = rest[:, :half] + below_left.astype(f32) + above_left.astype(f32)
    right = rest[:, half:] + below_right.astype(f32) + above_right.astype(f32)
    layer_out = jnp.concatenate([left, right], axis=1).astype(bf16)
    return (layer_out, new_state)


def solution(mesh):
    in_specs = (
        P(("grp", "ep"), None),
        P(None, ("grp", "ep"), "tp"),
        P(),
        P(None, "tp"),
        P("tp", None),
        P("tp", None),
        P("tp"),
        P(None, "tp", None, None),
        P(None, "tp", None, None),
        P("tp"),
        P("tp", None),
        P(),
        P("ep", None, "tp"),
        P("ep", None, "tp"),
        P("ep", "tp", None),
        P(None, "tp"),
        P(None, "tp"),
        P("tp", None),
        P(("grp", "ep"), None),
        P(("grp", "ep"), None),
    )
    out_specs = (P(("grp", "ep"), "tp"), P(None, ("grp", "ep"), "tp"))
    return jax.shard_map(body, mesh=mesh, in_specs=in_specs, out_specs=out_specs, check_vma=False)
```

profile of v0, /device:TPU:161, one launch (start us, length us, event | category | flops | bytes accessed | tf_op | source)
XLA Modules:
  0.0 194.8 jit_solution(9592766821075755313)
XLA Ops:
  0.7 7.4 %mixer.1 = (f32[2,96,2048]{2,1,0:T(8,128)}, bf16[96,2048]{1,0:T(8,128)(2,1)}) custom-call(bf16[96,2048]{1,0:T(8,128)(2,1)} %tok.3, f32[1,2048]{1,0:T(1,128)} %bitcast.39, bf16[2048,512]{1,0:T(8,128)(2,1)} %w_in.1, f32[2,96,2048]{2,1,0:T(8,128)} %state.1, f32[32,64]{1,0:T(8,128)} %decay.1, f32[32,64]{1,0:T(8,128)} %freq.1, f32[1,32]{1,0:T(1,128)} %bitcast.41, ...), custom_call_target="tpu_custom_call" | custom-call | tf_op jit(solution)/shard_map/mixer/pallas_call | solution.py:107
  8.1 0.7 collective-permute-start
  8.9 1.6 collective-permute-done.other
  10.6 1.5 shard_map.203
  12.1 10.5 %collective-permute-start.1 = (bf16[104,512]{1,0:T(8,128)(2,1)S(1)}, bf16[104,512]{1,0:T(8,128)(2,1)S(1)}, u32[]{:S(2)}, u32[]{:S(2)}) collective-permute-start(bf16[104,512]{1,0:T(8,128)(2,1)S(1)} %get-tuple-element.31.own_l), channel_id=1, source_target_pairs={{0,32},{1,33},{2,34},{3,35},{4,36},{5,37},{6,38},{7,39},{8,40},{9,... | collective-permute-start | bytes 319496 | tf_op jit(solution)/shard_map/ppermute | solution.py:323
  22.6 0.8 shard_map.205
  23.3 0.8 collective-permute-start.5
  24.1 9.4 %collective-permute-start.4 = (bf16[96,512]{1,0:T(8,128)(2,1)S(1)}, bf16[96,512]{1,0:T(8,128)(2,1)S(1)}, u32[]{:S(2)}, u32[]{:S(2)}) collective-permute-start(bf16[96,512]{1,0:T(8,128)(2,1)S(1)} %get-tuple-element.32.own_r), channel_id=1, source_target_pairs={{0,96},{1,97},{2,98},{3,99},{4,100},{5,101},{6,102},{7,103},{8,104... | collective-permute-start | bytes 294920 | tf_op jit(solution)/shard_map/ppermute | solution.py:323
  33.5 5.6 %collective-permute-start.3 = (bf16[104,512]{1,0:T(8,128)(2,1)S(1)}, bf16[104,512]{1,0:T(8,128)(2,1)S(1)}, u32[]{:S(2)}, u32[]{:S(2)}) collective-permute-start(bf16[104,512]{1,0:T(8,128)(2,1)S(1)} %get-tuple-element.31.own_l), channel_id=1, source_target_pairs={{0,96},{1,97},{2,98},{3,99},{4,100},{5,101},{6,102},{7,103},{8,104... | collective-permute-start | bytes 319496 | tf_op jit(solution)/shard_map/ppermute | solution.py:323
  39.6 6.1 %collective-permute-start.2 = (bf16[96,512]{1,0:T(8,128)(2,1)S(1)}, bf16[96,512]{1,0:T(8,128)(2,1)S(1)}, u32[]{:S(2)}, u32[]{:S(2)}) collective-permute-start(bf16[96,512]{1,0:T(8,128)(2,1)S(1)} %get-tuple-element.32.own_r), channel_id=1, source_target_pairs={{0,32},{1,33},{2,34},{3,35},{4,36},{5,37},{6,38},{7,39},{8,40},{9,... | collective-permute-start | bytes 294920 | tf_op jit(solution)/shard_map/ppermute | solution.py:323
  45.8 12.2 %collective-permute-done.2.below_r = bf16[96,512]{1,0:T(8,128)(2,1)S(1)} collective-permute-done((bf16[96,512]{1,0:T(8,128)(2,1)S(1)}, bf16[96,512]{1,0:T(8,128)(2,1)S(1)}, u32[]{:S(2)}, u32[]{:S(2)}) %collective-permute-start.2) | collective-permute-done | bytes 98336 | tf_op jit(solution)/shard_map/ppermute | solution.py:323
  58.0 1.9 shard_map.204
  59.9 0.8 shard_map.206
  60.8 48.0 %all_to_all.10 = bf16[16,56,1024]{2,1,0:T(8,128)(2,1)S(1)} all-to-all(bf16[16,56,1024]{2,1,0:T(8,128)(2,1)S(1)} %bitcast.32), channel_id=1, replica_groups={{0,2,4,6,8,10,12,14,16,18,20,22,24,26,28,30},{1,3,5,7,9,11,13,15,113,11..., dimensions={0} | all-to-all | bytes 3670016 | tf_op jit(solution)/shard_map/all_to_all | solution.py:342
  109.5 1.9 %collective-permute-done.10.other = bf16[448,1024]{1,0:T(8,128)(2,1)S(1)} collective-permute-done((bf16[448,1024]{1,0:T(8,128)(2,1)S(1)}, bf16[448,1024]{1,0:T(8,128)(2,1)S(1)}, u32[]{:S(2)}, u32[]{:S(2)}) %collective-permute-start.10) | collective-permute-done | bytes 917536 | tf_op jit(solution)/shard_map/ppermute | solution.py:328
  111.5 1.8 shard_map.208
  113.6 1.8 shard_map.207
  116.2 1.8 collective-permute-done.9
  118.5 39.1 %all_to_all.11 = bf16[16,56,1024]{2,1,0:T(8,128)(2,1)S(1)} all-to-all(bf16[16,56,1024]{2,1,0:T(8,128)(2,1)S(1)} %bitcast.34), channel_id=1, replica_groups={{0,2,4,6,8,10,12,14,16,18,20,22,24,26,28,30},{1,3,5,7,9,11,13,15,113,11..., dimensions={0} | all-to-all | bytes 3670016 | tf_op jit(solution)/shard_map/all_to_all | solution.py:342
  158.1 4.3 %collective-permute-start.12 = (bf16[96,512]{1,0:T(8,128)(2,1)S(1)}, bf16[96,512]{1,0:T(8,128)(2,1)S(1)}, u32[]{:S(2)}, u32[]{:S(2)}) collective-permute-start(bf16[96,512]{1,0:T(8,128)(2,1)S(1)} %get-tuple-element.50), channel_id=1, source_target_pairs={{0,32},{1,33},{2,34},{3,35},{4,36},{5,37},{6,38},{7,39},{8,40},{9,... | collective-permute-start | bytes 294920 | tf_op jit(solution)/shard_map/ppermute | solution.py:323
  162.4 1.1 shard_map.209
  163.5 1.3 collective-permute-start.16
  164.8 1.9 collective-permute-start.14
  166.7 3.5 %collective-permute-start.15 = (bf16[96,512]{1,0:T(8,128)(2,1)S(1)}, bf16[96,512]{1,0:T(8,128)(2,1)S(1)}, u32[]{:S(2)}, u32[]{:S(2)}) collective-permute-start(bf16[96,512]{1,0:T(8,128)(2,1)S(1)} %get-tuple-element.52), channel_id=1, source_target_pairs={{0,32},{1,33},{2,34},{3,35},{4,36},{5,37},{6,38},{7,39},{8,40},{9,... | collective-permute-start | bytes 294920 | tf_op jit(solution)/shard_map/ppermute | solution.py:323
  170.2 1.7 collective-permute-done.12
  171.9 2.7 %collective-permute-start.13 = (bf16[96,512]{1,0:T(8,128)(2,1)S(1)}, bf16[96,512]{1,0:T(8,128)(2,1)S(1)}, u32[]{:S(2)}, u32[]{:S(2)}) collective-permute-start(bf16[96,512]{1,0:T(8,128)(2,1)S(1)} %add_convert_fusion.3), channel_id=1, source_target_pairs={{0,32},{1,33},{2,34},{3,35},{4,36},{5,37},{6,38},{7,39},{8,40},{9,... | collective-permute-start | bytes 294920 | tf_op jit(solution)/shard_map/ppermute | solution.py:323
  174.5 6.1 %collective-permute-done.16 = bf16[96,512]{1,0:T(8,128)(2,1)S(1)} collective-permute-done((bf16[96,512]{1,0:T(8,128)(2,1)S(1)}, bf16[96,512]{1,0:T(8,128)(2,1)S(1)}, u32[]{:S(2)}, u32[]{:S(2)}) %collective-permute-start.16) | collective-permute-done | bytes 98336 | tf_op jit(solution)/shard_map/ppermute | solution.py:323
  180.7 1.2 collective-permute-start.17
  182.0 1.8 collective-permute-done.14
  183.8 4.6 %collective-permute-done.15 = bf16[96,512]{1,0:T(8,128)(2,1)S(1)} collective-permute-done((bf16[96,512]{1,0:T(8,128)(2,1)S(1)}, bf16[96,512]{1,0:T(8,128)(2,1)S(1)}, u32[]{:S(2)}, u32[]{:S(2)}) %collective-permute-start.15) | collective-permute-done | bytes 98336 | tf_op jit(solution)/shard_map/ppermute | solution.py:323
  188.4 2.1 %collective-permute-done.13 = bf16[96,512]{1,0:T(8,128)(2,1)S(1)} collective-permute-done((bf16[96,512]{1,0:T(8,128)(2,1)S(1)}, bf16[96,512]{1,0:T(8,128)(2,1)S(1)}, u32[]{:S(2)}, u32[]{:S(2)}) %collective-permute-start.13) | collective-permute-done | bytes 98336 | tf_op jit(solution)/shard_map/ppermute | solution.py:323
  190.5 3.5 %collective-permute-done.17 = bf16[96,512]{1,0:T(8,128)(2,1)S(1)} collective-permute-done((bf16[96,512]{1,0:T(8,128)(2,1)S(1)}, bf16[96,512]{1,0:T(8,128)(2,1)S(1)}, u32[]{:S(2)}, u32[]{:S(2)}) %collective-permute-start.17) | collective-permute-done | bytes 98336 | tf_op jit(solution)/shard_map/ppermute | solution.py:323
  (48 shorter events, 4.5 us)
Async XLA Ops:
  0.6 8.2 %copy-start.8 = (s32[96,6]{0,1:T(8,128)S(1)}, s32[96,6]{0,1:T(8,128)}, u32[]{:S(2)}) copy-start(s32[96,6]{0,1:T(8,128)} %param.38) | copy-start | bytes 6916
  0.6 8.2 %copy-start.9 = (f32[96,6]{0,1:T(8,128)S(1)}, f32[96,6]{0,1:T(8,128)}, u32[]{:S(2)}) copy-start(f32[96,6]{0,1:T(8,128)} %param.39) | copy-start | bytes 6916
  0.7 9.9 %copy-start.3 = (bf16[96,2048]{1,0:T(8,128)(2,1)S(1)}, bf16[96,2048]{1,0:T(8,128)(2,1)}, u32[]{:S(2)}) copy-start(bf16[96,2048]{1,0:T(8,128)(2,1)} %tok.3) | copy-start | bytes 1179652
  0.7 9.9 %copy-start.7 = (f32[2048]{0:T(1024)S(1)}, f32[2048]{0:T(1024)}, u32[]{:S(2)}) copy-start(f32[2048]{0:T(1024)} %param.31) | copy-start | bytes 24580
  0.7 21.9 %copy-start.5 = (bf16[2048,256]{1,0:T(8,128)(2,1)S(1)}, bf16[2048,256]{1,0:T(8,128)(2,1)}, u32[]{:S(2)}) copy-start(bf16[2048,256]{1,0:T(8,128)(2,1)} %up.1) | copy-start | bytes 3145732
  0.7 21.9 %copy-start.6 = (bf16[256,2048]{1,0:T(8,128)(2,1)S(1)}, bf16[256,2048]{1,0:T(8,128)(2,1)}, u32[]{:S(2)}) copy-start(bf16[256,2048]{1,0:T(8,128)(2,1)} %down.1) | copy-start | bytes 3145732
  8.1 14.4 %copy-start.4 = (bf16[2048,256]{1,0:T(8,128)(2,1)S(1)}, bf16[2048,256]{1,0:T(8,128)(2,1)}, u32[]{:S(2)}) copy-start(bf16[2048,256]{1,0:T(8,128)(2,1)} %gate.1) | copy-start | bytes 3145732
  8.1 2.4 %collective-permute-start = (bf16[96,2048]{1,0:T(8,128)(2,1)}, bf16[96,2048]{1,0:T(8,128)(2,1)}, u32[]{:S(2)}, u32[]{:S(2)}) collective-permute-start(bf16[96,2048]{1,0:T(8,128)(2,1)} %get-tuple-element.29.mine), channel_id=1, source_target_pairs={{0,1},{1,0},{2,3},{3,2},{4,5},{5,4},{6,7},{7,6},{8,9},{9,8},{10,11... | collective-permute-start | bytes 1179656 | tf_op jit(solution)/shard_map/ppermute | solution.py:328
  12.1 27.0 %collective-permute-start.1 = (bf16[104,512]{1,0:T(8,128)(2,1)S(1)}, bf16[104,512]{1,0:T(8,128)(2,1)S(1)}, u32[]{:S(2)}, u32[]{:S(2)}) collective-permute-start(bf16[104,512]{1,0:T(8,128)(2,1)S(1)} %get-tuple-element.31.own_l), channel_id=1, source_target_pairs={{0,32},{1,33},{2,34},{3,35},{4,36},{5,37},{6,38},{7,39},{8,40},{9,... | collective-permute-start | bytes 319496 | tf_op jit(solution)/shard_map/ppermute | solution.py:323
  23.3 36.6 %collective-permute-start.5 = (bf16[96,1024]{1,0:T(8,128)(2,1)S(1)}, bf16[96,1024]{1,0:T(8,128)(2,1)S(1)}, u32[]{:S(2)}, u32[]{:S(2)}) collective-permute-start(bf16[96,1024]{1,0:T(8,128)(2,1)S(1)} %get-tuple-element.37), channel_id=1, source_target_pairs={{0,1},{1,0},{2,3},{3,2},{4,5},{5,4},{6,7},{7,6},{8,9},{9,8},{10,11... | collective-permute-start | bytes 589832 | tf_op jit(solution)/shard_map/ppermute | solution.py:328
  24.1 21.6 %collective-permute-start.4 = (bf16[96,512]{1,0:T(8,128)(2,1)S(1)}, bf16[96,512]{1,0:T(8,128)(2,1)S(1)}, u32[]{:S(2)}, u32[]{:S(2)}) collective-permute-start(bf16[96,512]{1,0:T(8,128)(2,1)S(1)} %get-tuple-element.32.own_r), channel_id=1, source_target_pairs={{0,96},{1,97},{2,98},{3,99},{4,100},{5,101},{6,102},{7,103},{8,104... | collective-permute-start | bytes 294920 | tf_op jit(solution)/shard_map/ppermute | solution.py:323
  33.5 24.5 %collective-permute-start.3 = (bf16[104,512]{1,0:T(8,128)(2,1)S(1)}, bf16[104,512]{1,0:T(8,128)(2,1)S(1)}, u32[]{:S(2)}, u32[]{:S(2)}) collective-permute-start(bf16[104,512]{1,0:T(8,128)(2,1)S(1)} %get-tuple-element.31.own_l), channel_id=1, source_target_pairs={{0,96},{1,97},{2,98},{3,99},{4,100},{5,101},{6,102},{7,103},{8,104... | collective-permute-start | bytes 319496 | tf_op jit(solution)/shard_map/ppermute | solution.py:323
  39.1 20.9 %collective-permute-start.6 = (bf16[104,512]{1,0:T(8,128)(2,1)S(1)}, bf16[104,512]{1,0:T(8,128)(2,1)S(1)}, u32[]{:S(2)}, u32[]{:S(2)}) collective-permute-start(bf16[104,512]{1,0:T(8,128)(2,1)S(1)} %collective-permute-done.1.below_l), channel_id=1, source_target_pairs={{0,32},{1,33},{2,34},{3,35},{4,36},{5,37},{6,38},{7,39},{8,40},{9,... | collective-permute-start | bytes 319496 | tf_op jit(solution)/shard_map/ppermute | solution.py:323
  39.6 18.4 %collective-permute-start.2 = (bf16[96,512]{1,0:T(8,128)(2,1)S(1)}, bf16[96,512]{1,0:T(8,128)(2,1)S(1)}, u32[]{:S(2)}, u32[]{:S(2)}) collective-permute-start(bf16[96,512]{1,0:T(8,128)(2,1)S(1)} %get-tuple-element.32.own_r), channel_id=1, source_target_pairs={{0,32},{1,33},{2,34},{3,35},{4,36},{5,37},{6,38},{7,39},{8,40},{9,... | collective-permute-start | bytes 294920 | tf_op jit(solution)/shard_map/ppermute | solution.py:323
  45.7 14.2 %collective-permute-start.7 = (bf16[96,512]{1,0:T(8,128)(2,1)S(1)}, bf16[96,512]{1,0:T(8,128)(2,1)S(1)}, u32[]{:S(2)}, u32[]{:S(2)}) collective-permute-start(bf16[96,512]{1,0:T(8,128)(2,1)S(1)} %collective-permute-done.4.above_r), channel_id=1, source_target_pairs={{0,96},{1,97},{2,98},{3,99},{4,100},{5,101},{6,102},{7,103},{8,104... | collective-permute-start | bytes 294920 | tf_op jit(solution)/shard_map/ppermute | solution.py:323
  108.7 2.8 %copy-start = (bf16[1,2048,256]{2,1,0:T(8,128)(2,1)S(1)}, bf16[1,2048,256]{2,1,0:T(8,128)(2,1)}, u32[]{:S(2)}) copy-start(bf16[1,2048,256]{2,1,0:T(8,128)(2,1)} %param.32) | copy-start | bytes 3145732
  108.7 2.8 %copy-start.1 = (bf16[1,2048,256]{2,1,0:T(8,128)(2,1)S(1)}, bf16[1,2048,256]{2,1,0:T(8,128)(2,1)}, u32[]{:S(2)}) copy-start(bf16[1,2048,256]{2,1,0:T(8,128)(2,1)} %param.33) | copy-start | bytes 3145732
  108.7 2.8 %copy-start.2 = (bf16[1,256,2048]{2,1,0:T(8,128)(2,1)S(1)}, bf16[1,256,2048]{2,1,0:T(8,128)(2,1)}, u32[]{:S(2)}) copy-start(bf16[1,256,2048]{2,1,0:T(8,128)(2,1)} %param.34) | copy-start | bytes 3145732
  108.9 2.6 %collective-permute-start.10 = (bf16[448,1024]{1,0:T(8,128)(2,1)S(1)}, bf16[448,1024]{1,0:T(8,128)(2,1)S(1)}, u32[]{:S(2)}, u32[]{:S(2)}) collective-permute-start(bf16[448,1024]{1,0:T(8,128)(2,1)S(1)} %bitcast.36), channel_id=1, source_target_pairs={{0,1},{1,0},{2,3},{3,2},{4,5},{5,4},{6,7},{7,6},{8,9},{9,8},{10,11... | collective-permute-start | bytes 2752520 | tf_op jit(solution)/shard_map/ppermute | solution.py:328
  109.2 4.4 %collective-permute-start.8 = (bf16[448,1024]{1,0:T(8,128)(2,1)S(1)}, bf16[448,1024]{1,0:T(8,128)(2,1)S(1)}, u32[]{:S(2)}, u32[]{:S(2)}) collective-permute-start(bf16[448,1024]{1,0:T(8,128)(2,1)S(1)} %bitcast.35), channel_id=1, source_target_pairs={{0,1},{1,0},{2,3},{3,2},{4,5},{5,4},{6,7},{7,6},{8,9},{9,8},{10,11... | collective-permute-start | bytes 2752520 | tf_op jit(solution)/shard_map/ppermute | solution.py:328
  113.3 2.6 %collective-permute-start.11 = (bf16[448,1024]{1,0:T(8,128)(2,1)S(1)}, bf16[448,1024]{1,0:T(8,128)(2,1)S(1)}, u32[]{:S(2)}, u32[]{:S(2)}) collective-permute-start(bf16[448,1024]{1,0:T(8,128)(2,1)S(1)} %get-tuple-element.46), channel_id=1, source_target_pairs={{0,1},{1,0},{2,3},{3,2},{4,5},{5,4},{6,7},{7,6},{8,9},{9,8},{10,11... | collective-permute-start | bytes 2752520 | tf_op jit(solution)/shard_map/ppermute | solution.py:328
  115.4 2.6 %collective-permute-start.9 = (bf16[448,1024]{1,0:T(8,128)(2,1)S(1)}, bf16[448,1024]{1,0:T(8,128)(2,1)S(1)}, u32[]{:S(2)}, u32[]{:S(2)}) collective-permute-start(bf16[448,1024]{1,0:T(8,128)(2,1)S(1)} %get-tuple-element.44), channel_id=1, source_target_pairs={{0,1},{1,0},{2,3},{3,2},{4,5},{5,4},{6,7},{7,6},{8,9},{9,8},{10,11... | collective-permute-start | bytes 2752520 | tf_op jit(solution)/shard_map/ppermute | solution.py:328
  158.1 13.7 %collective-permute-start.12 = (bf16[96,512]{1,0:T(8,128)(2,1)S(1)}, bf16[96,512]{1,0:T(8,128)(2,1)S(1)}, u32[]{:S(2)}, u32[]{:S(2)}) collective-permute-start(bf16[96,512]{1,0:T(8,128)(2,1)S(1)} %get-tuple-element.50), channel_id=1, source_target_pairs={{0,32},{1,33},{2,34},{3,35},{4,36},{5,37},{6,38},{7,39},{8,40},{9,... | collective-permute-start | bytes 294920 | tf_op jit(solution)/shard_map/ppermute | solution.py:323
  163.5 17.1 %collective-permute-start.16 = (bf16[96,512]{1,0:T(8,128)(2,1)S(1)}, bf16[96,512]{1,0:T(8,128)(2,1)S(1)}, u32[]{:S(2)}, u32[]{:S(2)}) collective-permute-start(bf16[96,512]{1,0:T(8,128)(2,1)S(1)} %get-tuple-element.54), channel_id=1, source_target_pairs={{0,96},{1,97},{2,98},{3,99},{4,100},{5,101},{6,102},{7,103},{8,104... | collective-permute-start | bytes 294920 | tf_op jit(solution)/shard_map/ppermute | solution.py:323
  164.8 18.9 %collective-permute-start.14 = (bf16[96,512]{1,0:T(8,128)(2,1)S(1)}, bf16[96,512]{1,0:T(8,128)(2,1)S(1)}, u32[]{:S(2)}, u32[]{:S(2)}) collective-permute-start(bf16[96,512]{1,0:T(8,128)(2,1)S(1)} %get-tuple-element.51), channel_id=1, source_target_pairs={{0,96},{1,97},{2,98},{3,99},{4,100},{5,101},{6,102},{7,103},{8,104... | collective-permute-start | bytes 294920 | tf_op jit(solution)/shard_map/ppermute | solution.py:323
  166.7 21.6 %collective-permute-start.15 = (bf16[96,512]{1,0:T(8,128)(2,1)S(1)}, bf16[96,512]{1,0:T(8,128)(2,1)S(1)}, u32[]{:S(2)}, u32[]{:S(2)}) collective-permute-start(bf16[96,512]{1,0:T(8,128)(2,1)S(1)} %get-tuple-element.52), channel_id=1, source_target_pairs={{0,32},{1,33},{2,34},{3,35},{4,36},{5,37},{6,38},{7,39},{8,40},{9,... | collective-permute-start | bytes 294920 | tf_op jit(solution)/shard_map/ppermute | solution.py:323
  171.9 18.6 %collective-permute-start.13 = (bf16[96,512]{1,0:T(8,128)(2,1)S(1)}, bf16[96,512]{1,0:T(8,128)(2,1)S(1)}, u32[]{:S(2)}, u32[]{:S(2)}) collective-permute-start(bf16[96,512]{1,0:T(8,128)(2,1)S(1)} %add_convert_fusion.3), channel_id=1, source_target_pairs={{0,32},{1,33},{2,34},{3,35},{4,36},{5,37},{6,38},{7,39},{8,40},{9,... | collective-permute-start | bytes 294920 | tf_op jit(solution)/shard_map/ppermute | solution.py:323
  180.7 13.3 %collective-permute-start.17 = (bf16[96,512]{1,0:T(8,128)(2,1)S(1)}, bf16[96,512]{1,0:T(8,128)(2,1)S(1)}, u32[]{:S(2)}, u32[]{:S(2)}) collective-permute-start(bf16[96,512]{1,0:T(8,128)(2,1)S(1)} %add_convert_fusion.2), channel_id=1, source_target_pairs={{0,96},{1,97},{2,98},{3,99},{4,100},{5,101},{6,102},{7,103},{8,104... | collective-permute-start | bytes 294920 | tf_op jit(solution)/shard_map/ppermute | solution.py:323
where the time goes:
time: 195 us
  blocking collectives  87.1 us (45%)
  starting transfers between devices  49.9 us (26%)
  waiting for transfers between devices  37.4 us (19%)
  Pallas kernels  17.6 us (9%)
    all_to_all x2, blocking collectives, exchange(): lax.all_to_all(tiles, AXES, 0, 0, axis_index_groups=nearby, tiled=True)  87.1 us
    ppermute x12, starting transfers between devices, along(): lax.ppermute(value, AXES, [(at(z, x, t), at(z + offset, x, t)) for z, x,...  47 us
    ppermute x12, waiting for transfers between devices, along(): lax.ppermute(value, AXES, [(at(z, x, t), at(z + offset, x, t)) for z, x,...  32 us
    pallas_call x8, Pallas kernels, call(): pl.pallas_call(kernel, in_specs=[SM] + [VM] * len(arrays), out_specs=[VM]...  10.1 us
    pallas_call x1, Pallas kernels, mixer(): pl.pallas_call(mixer_kernel, grid=(steps,), in_specs=[VM, pl.BlockSpec((1...  7.43 us
    ppermute x6, waiting for transfers between devices, swap(): return lax.ppermute(value, 'tp', [(t, cores - 1 - t) for t in range(cores)])  5.39 us
  transfers between devices with their start and end apart: 18, of which 10 were waited for; matrix products, arithmetic and copies ran while one was open for 0% of the time, Pallas kernels for 4%

commit v1 on v0

--- a/solution.py
+++ b/solution.py
@@ -217,8 +217,9 @@
         hits = hits + hit
         weight = weight + hit * table[k : k + 1, LANES : LANES + rows]
     rank = dot(hits.astype(bf16), before)
-    home = plane - NEAR * m
-    home = jnp.where(home < 0, home + planes, home) // NEAR
+    home = plane // NEAR
+    clusters = planes // NEAR
+    home = (home, home + 1 - 2 * (home % 2), (home + clusters // 2) % clusters, clusters - 1 - home)[m]
     place = jnp.where(hits > 0.5, rank + (home * cap).astype(f32), -1.0)
     for d in range(0, dests, 2):
         ones = [(level == place[e : e + 1, :]).astype(f32) for e in (d, d + 1)]
@@ -319,10 +320,12 @@
 
     everyone = [(z, x, t) for z in range(planes) for x in range(RING) for t in range(cores)]
 
-    def along(value, offset):
-        return lax.ppermute(
-            value, AXES, [(at(z, x, t), at(z + offset, x, t)) for z, x, t in everyone]
-        )
+    def pair(value, shift):
+        def mate(z):
+            up = (z // NEAR + shift) % 2 == 0
+            return z + NEAR if up else z - NEAR
+
+        return lax.ppermute(value, AXES, [(at(z, x, t), at(mate(z), x, t)) for z, x, t in everyone])
 
     def swap(value):
         return lax.ppermute(value, "tp", [(t, cores - 1 - t) for t in range(cores)])
@@ -371,9 +374,9 @@
         spot, tokens, partial, swap(partial), channel_gain[None], table
     )
 
-    below_l, above_r = along(own_l, NEAR), along(own_r, -NEAR)
-    below_r, above_l = along(own_r, NEAR), along(own_l, -NEAR)
-    far_l, far_r = along(below_l, NEAR), along(above_r, -NEAR)
+    below_l, above_r = pair(own_l, 0), pair(own_r, 1)
+    below_r, above_l = pair(own_r, 0), pair(own_l, 1)
+    far_l, far_r = pair(below_l, 1), pair(above_r, 0)
     shared_keep, shared_send = block(spot, own, other, shared_gate, shared_up, shared_down, 0)
     shared_recv = swap(shared_send)
     sizes = (slot_cap, planes, slots)
@@ -403,13 +406,13 @@
 
     sent, sums = ((seq_rows, half), bf16), ((seq_rows, half), f32)
     m_far_l, m_far_r = call(mix_far_kernel, spot, (mix_far, back), [sent] * 2)
-    in_l, in_r = along(m_far_l, NEAR), along(m_far_r, -NEAR)
+    in_l, in_r = pair(m_far_l, 0), pair(m_far_r, 1)
     m_own, m_below_l, m_below_r, m_above_l, m_above_r = call(
         mix_near_kernel, spot, (mix_near, back), [((seq_rows, wide), f32), sent, sums, sums, sent]
     )
-    below_right, above_left = along(m_above_r, NEAR), along(m_below_l, -NEAR)
-    below_left = along((m_above_l + in_l.astype(f32)).astype(bf16), NEAR)
-    above_right = along((m_below_r + in_r.astype(f32)).astype(bf16), -NEAR)
+    above_right, below_left = pair(m_above_r, 1), pair(m_below_l, 0)
+    above_left = pair((m_above_l + in_l.astype(f32)).astype(bf16), 1)
+    below_right = pair((m_below_r + in_r.astype(f32)).astype(bf16), 0)
     shared_out = shared_keep.astype(f32) + shared_recv.astype(f32)
     rest = middle.astype(f32) + shared_out + m_own
     left = rest[:, :half] + below_left.astype(f32) + above_left.astype(f32)

time: 195 us -> 198 us (1.015)
  the two profiles are of different devices: /device:TPU:161 before, /device:TPU:34 now
where the time goes in v1:
time: 198 us; the launch traced here: 196 us
  blocking collectives  88.1 us (44%)
  starting transfers between devices  63.8 us (32%)
  waiting for transfers between devices  24 us (12%)
  Pallas kernels  17.6 us (9%)
    all_to_all x2, blocking collectives, exchange(): lax.all_to_all(tiles, AXES, 0, 0, axis_index_groups=nearby, tiled=True)  88.1 us
    ppermute x12, starting transfers between devices, pair(): lax.ppermute(value, AXES, [(at(z, x, t), at(mate(z), x, t)) for z, x, t i...  62.1 us
    ppermute x12, waiting for transfers between devices, pair(): lax.ppermute(value, AXES, [(at(z, x, t), at(mate(z), x, t)) for z, x, t i...  18.3 us
    pallas_call x8, Pallas kernels, call(): pl.pallas_call(kernel, in_specs=[SM] + [VM] * len(arrays), out_specs=[VM]...  10.1 us
    pallas_call x1, Pallas kernels, mixer(): pl.pallas_call(mixer_kernel, grid=(steps,), in_specs=[VM, pl.BlockSpec((1...  7.43 us
    ppermute x6, waiting for transfers between devices, swap(): return lax.ppermute(value, 'tp', [(t, cores - 1 - t) for t in range(cores)])  5.67 us
  transfers between devices with their start and end apart: 18, of which 12 were waited for; matrix products, arithmetic and copies ran while one was open for 0% of the time, Pallas kernels for 4%

profile of v1, /device:TPU:34, one launch (start us, length us, event | category | flops | bytes accessed | tf_op | source)
XLA Modules:
  0.0 196.3 jit_solution(5189961011311959601)
XLA Ops:
  0.7 7.4 %mixer.1 = (f32[2,96,2048]{2,1,0:T(8,128)}, bf16[96,2048]{1,0:T(8,128)(2,1)}) custom-call(bf16[96,2048]{1,0:T(8,128)(2,1)} %tok.3, f32[1,2048]{1,0:T(1,128)} %bitcast.39, bf16[2048,512]{1,0:T(8,128)(2,1)} %w_in.1, f32[2,96,2048]{2,1,0:T(8,128)} %state.1, f32[32,64]{1,0:T(8,128)} %decay.1, f32[32,64]{1,0:T(8,128)} %freq.1, f32[1,32]{1,0:T(1,128)} %bitcast.41, ...), custom_call_target="tpu_custom_call" | custom-call | tf_op jit(solution)/shard_map/mixer/pallas_call | solution.py:107
  8.4 2.0 collective-permute-done.other
  10.3 1.5 shard_map.203
  11.8 10.8 %collective-permute-start.1 = (bf16[104,512]{1,0:T(8,128)(2,1)S(1)}, bf16[104,512]{1,0:T(8,128)(2,1)S(1)}, u32[]{:S(2)}, u32[]{:S(2)}) collective-permute-start(bf16[104,512]{1,0:T(8,128)(2,1)S(1)} %get-tuple-element.31.own_l), channel_id=1, source_target_pairs={{0,32},{1,33},{2,34},{3,35},{4,36},{5,37},{6,38},{7,39},{8,40},{9,... | collective-permute-start | bytes 319496 | tf_op jit(solution)/shard_map/ppermute | solution.py:328
  22.6 0.8 shard_map.205
  23.5 10.7 %collective-permute-start.4 = (bf16[96,512]{1,0:T(8,128)(2,1)S(1)}, bf16[96,512]{1,0:T(8,128)(2,1)S(1)}, u32[]{:S(2)}, u32[]{:S(2)}) collective-permute-start(bf16[96,512]{1,0:T(8,128)(2,1)S(1)} %get-tuple-element.32.own_r), channel_id=1, source_target_pairs={{0,96},{1,97},{2,98},{3,99},{4,100},{5,101},{6,102},{7,103},{8,104... | collective-permute-start | bytes 294920 | tf_op jit(solution)/shard_map/ppermute | solution.py:328
  34.4 7.9 %collective-permute-start.6 = (bf16[104,512]{1,0:T(8,128)(2,1)S(1)}, bf16[104,512]{1,0:T(8,128)(2,1)S(1)}, u32[]{:S(2)}, u32[]{:S(2)}) collective-permute-start(bf16[104,512]{1,0:T(8,128)(2,1)S(1)} %collective-permute-done.1.below_l), channel_id=1, source_target_pairs={{0,96},{1,97},{2,98},{3,99},{4,100},{5,101},{6,102},{7,103},{8,104... | collective-permute-start | bytes 319496 | tf_op jit(solution)/shard_map/ppermute | solution.py:328
  42.3 5.3 %collective-permute-start.2 = (bf16[96,512]{1,0:T(8,128)(2,1)S(1)}, bf16[96,512]{1,0:T(8,128)(2,1)S(1)}, u32[]{:S(2)}, u32[]{:S(2)}) collective-permute-start(bf16[96,512]{1,0:T(8,128)(2,1)S(1)} %get-tuple-element.32.own_r), channel_id=1, source_target_pairs={{0,32},{1,33},{2,34},{3,35},{4,36},{5,37},{6,38},{7,39},{8,40},{9,... | collective-permute-start | bytes 294920 | tf_op jit(solution)/shard_map/ppermute | solution.py:328
  47.7 5.5 %collective-permute-start.7 = (bf16[96,512]{1,0:T(8,128)(2,1)S(1)}, bf16[96,512]{1,0:T(8,128)(2,1)S(1)}, u32[]{:S(2)}, u32[]{:S(2)}) collective-permute-start(bf16[96,512]{1,0:T(8,128)(2,1)S(1)} %collective-permute-done.4.above_r), channel_id=1, source_target_pairs={{0,32},{1,33},{2,34},{3,35},{4,36},{5,37},{6,38},{7,39},{8,40},{9,... | collective-permute-start | bytes 294920 | tf_op jit(solution)/shard_map/ppermute | solution.py:328
  53.3 2.0 collective-permute-done.2.below_r
  55.2 1.8 collective-permute-done.3.above_l
  57.0 1.9 shard_map.204
  58.9 2.9 %collective-permute-done.7.far_r = bf16[96,512]{1,0:T(8,128)(2,1)S(1)} collective-permute-done((bf16[96,512]{1,0:T(8,128)(2,1)S(1)}, bf16[96,512]{1,0:T(8,128)(2,1)S(1)}, u32[]{:S(2)}, u32[]{:S(2)}) %collective-permute-start.7) | collective-permute-done | bytes 98336 | tf_op jit(solution)/shard_map/ppermute | solution.py:328
  61.9 0.8 shard_map.206
  62.7 47.7 %all_to_all.10 = bf16[16,56,1024]{2,1,0:T(8,128)(2,1)S(1)} all-to-all(bf16[16,56,1024]{2,1,0:T(8,128)(2,1)S(1)} %bitcast.32), channel_id=1, replica_groups={{0,2,4,6,8,10,12,14,16,18,20,22,24,26,28,30},{1,3,5,7,9,11,13,15,113,11..., dimensions={0} | all-to-all | bytes 3670016 | tf_op jit(solution)/shard_map/all_to_all | solution.py:345
  111.2 2.0 collective-permute-done.10.other
  113.2 1.8 shard_map.208
  115.2 1.8 shard_map.207
  117.9 1.7 collective-permute-done.9
  120.1 40.4 %all_to_all.11 = bf16[16,56,1024]{2,1,0:T(8,128)(2,1)S(1)} all-to-all(bf16[16,56,1024]{2,1,0:T(8,128)(2,1)S(1)} %bitcast.34), channel_id=1, replica_groups={{0,2,4,6,8,10,12,14,16,18,20,22,24,26,28,30},{1,3,5,7,9,11,13,15,113,11..., dimensions={0} | all-to-all | bytes 3670016 | tf_op jit(solution)/shard_map/all_to_all | solution.py:345
  161.0 4.7 %collective-permute-start.13 = (bf16[96,512]{1,0:T(8,128)(2,1)S(1)}, bf16[96,512]{1,0:T(8,128)(2,1)S(1)}, u32[]{:S(2)}, u32[]{:S(2)}) collective-permute-start(bf16[96,512]{1,0:T(8,128)(2,1)S(1)} %get-tuple-element.51), channel_id=1, source_target_pairs={{0,32},{1,33},{2,34},{3,35},{4,36},{5,37},{6,38},{7,39},{8,40},{9,... | collective-permute-start | bytes 294920 | tf_op jit(solution)/shard_map/ppermute | solution.py:328
  165.7 1.1 shard_map.209
  166.8 2.7 %collective-permute-start.15 = (bf16[96,512]{1,0:T(8,128)(2,1)S(1)}, bf16[96,512]{1,0:T(8,128)(2,1)S(1)}, u32[]{:S(2)}, u32[]{:S(2)}) collective-permute-start(bf16[96,512]{1,0:T(8,128)(2,1)S(1)} %get-tuple-element.53), channel_id=1, source_target_pairs={{0,96},{1,97},{2,98},{3,99},{4,100},{5,101},{6,102},{7,103},{8,104... | collective-permute-start | bytes 294920 | tf_op jit(solution)/shard_map/ppermute | solution.py:328
  169.5 1.3 collective-permute-start.12
  170.7 3.5 %collective-permute-start.17 = (bf16[96,512]{1,0:T(8,128)(2,1)S(1)}, bf16[96,512]{1,0:T(8,128)(2,1)S(1)}, u32[]{:S(2)}, u32[]{:S(2)}) collective-permute-start(bf16[96,512]{1,0:T(8,128)(2,1)S(1)} %get-tuple-element.54), channel_id=1, source_target_pairs={{0,96},{1,97},{2,98},{3,99},{4,100},{5,101},{6,102},{7,103},{8,104... | collective-permute-start | bytes 294920 | tf_op jit(solution)/shard_map/ppermute | solution.py:328
  174.4 4.6 %collective-permute-start.14 = (bf16[96,512]{1,0:T(8,128)(2,1)S(1)}, bf16[96,512]{1,0:T(8,128)(2,1)S(1)}, u32[]{:S(2)}, u32[]{:S(2)}) collective-permute-start(bf16[96,512]{1,0:T(8,128)(2,1)S(1)} %add_convert_fusion.3), channel_id=1, source_target_pairs={{0,96},{1,97},{2,98},{3,99},{4,100},{5,101},{6,102},{7,103},{8,104... | collective-permute-start | bytes 294920 | tf_op jit(solution)/shard_map/ppermute | solution.py:328
  179.0 2.3 %collective-permute-done.15 = bf16[96,512]{1,0:T(8,128)(2,1)S(1)} collective-permute-done((bf16[96,512]{1,0:T(8,128)(2,1)S(1)}, bf16[96,512]{1,0:T(8,128)(2,1)S(1)}, u32[]{:S(2)}, u32[]{:S(2)}) %collective-permute-start.15) | collective-permute-done | bytes 98336 | tf_op jit(solution)/shard_map/ppermute | solution.py:328
  181.3 5.0 %collective-permute-start.16 = (bf16[96,512]{1,0:T(8,128)(2,1)S(1)}, bf16[96,512]{1,0:T(8,128)(2,1)S(1)}, u32[]{:S(2)}, u32[]{:S(2)}) collective-permute-start(bf16[96,512]{1,0:T(8,128)(2,1)S(1)} %add_convert_fusion.2), channel_id=1, source_target_pairs={{0,32},{1,33},{2,34},{3,35},{4,36},{5,37},{6,38},{7,39},{8,40},{9,... | collective-permute-start | bytes 294920 | tf_op jit(solution)/shard_map/ppermute | solution.py:328
  186.4 1.8 collective-permute-done.17
  188.2 3.0 %collective-permute-done.14 = bf16[96,512]{1,0:T(8,128)(2,1)S(1)} collective-permute-done((bf16[96,512]{1,0:T(8,128)(2,1)S(1)}, bf16[96,512]{1,0:T(8,128)(2,1)S(1)}, u32[]{:S(2)}, u32[]{:S(2)}) %collective-permute-start.14) | collective-permute-done | bytes 98336 | tf_op jit(solution)/shard_map/ppermute | solution.py:328
  191.3 4.2 %collective-permute-done.16 = bf16[96,512]{1,0:T(8,128)(2,1)S(1)} collective-permute-done((bf16[96,512]{1,0:T(8,128)(2,1)S(1)}, bf16[96,512]{1,0:T(8,128)(2,1)S(1)}, u32[]{:S(2)}, u32[]{:S(2)}) %collective-permute-start.16) | collective-permute-done | bytes 98336 | tf_op jit(solution)/shard_map/ppermute | solution.py:328
  195.6 0.7 pad_maximum_fusion.1
  (48 shorter events, 3.8 us)
Async XLA Ops:
  0.6 7.7 %copy-start.8 = (s32[96,6]{0,1:T(8,128)S(1)}, s32[96,6]{0,1:T(8,128)}, u32[]{:S(2)}) copy-start(s32[96,6]{0,1:T(8,128)} %param.38) | copy-start | bytes 6916
  0.6 7.7 %copy-start.9 = (f32[96,6]{0,1:T(8,128)S(1)}, f32[96,6]{0,1:T(8,128)}, u32[]{:S(2)}) copy-start(f32[96,6]{0,1:T(8,128)} %param.39) | copy-start | bytes 6916
  0.7 9.7 %copy-start.3 = (bf16[96,2048]{1,0:T(8,128)(2,1)S(1)}, bf16[96,2048]{1,0:T(8,128)(2,1)}, u32[]{:S(2)}) copy-start(bf16[96,2048]{1,0:T(8,128)(2,1)} %tok.3) | copy-start | bytes 1179652
  0.7 9.7 %copy-start.7 = (f32[2048]{0:T(1024)S(1)}, f32[2048]{0:T(1024)}, u32[]{:S(2)}) copy-start(f32[2048]{0:T(1024)} %param.31) | copy-start | bytes 24580
  0.7 21.9 %copy-start.5 = (bf16[2048,256]{1,0:T(8,128)(2,1)S(1)}, bf16[2048,256]{1,0:T(8,128)(2,1)}, u32[]{:S(2)}) copy-start(bf16[2048,256]{1,0:T(8,128)(2,1)} %up.1) | copy-start | bytes 3145732
  0.7 21.9 %copy-start.6 = (bf16[256,2048]{1,0:T(8,128)(2,1)S(1)}, bf16[256,2048]{1,0:T(8,128)(2,1)}, u32[]{:S(2)}) copy-start(bf16[256,2048]{1,0:T(8,128)(2,1)} %down.1) | copy-start | bytes 3145732
  8.1 14.5 %copy-start.4 = (bf16[2048,256]{1,0:T(8,128)(2,1)S(1)}, bf16[2048,256]{1,0:T(8,128)(2,1)}, u32[]{:S(2)}) copy-start(bf16[2048,256]{1,0:T(8,128)(2,1)} %gate.1) | copy-start | bytes 3145732
  8.1 2.2 %collective-permute-start = (bf16[96,2048]{1,0:T(8,128)(2,1)}, bf16[96,2048]{1,0:T(8,128)(2,1)}, u32[]{:S(2)}, u32[]{:S(2)}) collective-permute-start(bf16[96,2048]{1,0:T(8,128)(2,1)} %get-tuple-element.29.mine), channel_id=1, source_target_pairs={{0,1},{1,0},{2,3},{3,2},{4,5},{5,4},{6,7},{7,6},{8,9},{9,8},{10,11... | collective-permute-start | bytes 1179656 | tf_op jit(solution)/shard_map/ppermute | solution.py:331
  11.8 22.6 %collective-permute-start.1 = (bf16[104,512]{1,0:T(8,128)(2,1)S(1)}, bf16[104,512]{1,0:T(8,128)(2,1)S(1)}, u32[]{:S(2)}, u32[]{:S(2)}) collective-permute-start(bf16[104,512]{1,0:T(8,128)(2,1)S(1)} %get-tuple-element.31.own_l), channel_id=1, source_target_pairs={{0,32},{1,33},{2,34},{3,35},{4,36},{5,37},{6,38},{7,39},{8,40},{9,... | collective-permute-start | bytes 319496 | tf_op jit(solution)/shard_map/ppermute | solution.py:328
  23.4 35.6 %collective-permute-start.5 = (bf16[96,1024]{1,0:T(8,128)(2,1)S(1)}, bf16[96,1024]{1,0:T(8,128)(2,1)S(1)}, u32[]{:S(2)}, u32[]{:S(2)}) collective-permute-start(bf16[96,1024]{1,0:T(8,128)(2,1)S(1)} %get-tuple-element.37), channel_id=1, source_target_pairs={{0,1},{1,0},{2,3},{3,2},{4,5},{5,4},{6,7},{7,6},{8,9},{9,8},{10,11... | collective-permute-start | bytes 589832 | tf_op jit(solution)/shard_map/ppermute | solution.py:331
  23.5 24.2 %collective-permute-start.4 = (bf16[96,512]{1,0:T(8,128)(2,1)S(1)}, bf16[96,512]{1,0:T(8,128)(2,1)S(1)}, u32[]{:S(2)}, u32[]{:S(2)}) collective-permute-start(bf16[96,512]{1,0:T(8,128)(2,1)S(1)} %get-tuple-element.32.own_r), channel_id=1, source_target_pairs={{0,96},{1,97},{2,98},{3,99},{4,100},{5,101},{6,102},{7,103},{8,104... | collective-permute-start | bytes 294920 | tf_op jit(solution)/shard_map/ppermute | solution.py:328
  34.2 22.8 %collective-permute-start.3 = (bf16[104,512]{1,0:T(8,128)(2,1)S(1)}, bf16[104,512]{1,0:T(8,128)(2,1)S(1)}, u32[]{:S(2)}, u32[]{:S(2)}) collective-permute-start(bf16[104,512]{1,0:T(8,128)(2,1)S(1)} %get-tuple-element.31.own_l), channel_id=1, source_target_pairs={{0,96},{1,97},{2,98},{3,99},{4,100},{5,101},{6,102},{7,103},{8,104... | collective-permute-start | bytes 319496 | tf_op jit(solution)/shard_map/ppermute | solution.py:328
  34.4 27.5 %collective-permute-start.6 = (bf16[104,512]{1,0:T(8,128)(2,1)S(1)}, bf16[104,512]{1,0:T(8,128)(2,1)S(1)}, u32[]{:S(2)}, u32[]{:S(2)}) collective-permute-start(bf16[104,512]{1,0:T(8,128)(2,1)S(1)} %collective-permute-done.1.below_l), channel_id=1, source_target_pairs={{0,96},{1,97},{2,98},{3,99},{4,100},{5,101},{6,102},{7,103},{8,104... | collective-permute-start | bytes 319496 | tf_op jit(solution)/shard_map/ppermute | solution.py:328
  42.3 12.9 %collective-permute-start.2 = (bf16[96,512]{1,0:T(8,128)(2,1)S(1)}, bf16[96,512]{1,0:T(8,128)(2,1)S(1)}, u32[]{:S(2)}, u32[]{:S(2)}) collective-permute-start(bf16[96,512]{1,0:T(8,128)(2,1)S(1)} %get-tuple-element.32.own_r), channel_id=1, source_target_pairs={{0,32},{1,33},{2,34},{3,35},{4,36},{5,37},{6,38},{7,39},{8,40},{9,... | collective-permute-start | bytes 294920 | tf_op jit(solution)/shard_map/ppermute | solution.py:328
  47.7 14.2 %collective-permute-start.7 = (bf16[96,512]{1,0:T(8,128)(2,1)S(1)}, bf16[96,512]{1,0:T(8,128)(2,1)S(1)}, u32[]{:S(2)}, u32[]{:S(2)}) collective-permute-start(bf16[96,512]{1,0:T(8,128)(2,1)S(1)} %collective-permute-done.4.above_r), channel_id=1, source_target_pairs={{0,32},{1,33},{2,34},{3,35},{4,36},{5,37},{6,38},{7,39},{8,40},{9,... | collective-permute-start | bytes 294920 | tf_op jit(solution)/shard_map/ppermute | solution.py:328
  110.4 2.8 %copy-start = (bf16[1,2048,256]{2,1,0:T(8,128)(2,1)S(1)}, bf16[1,2048,256]{2,1,0:T(8,128)(2,1)}, u32[]{:S(2)}) copy-start(bf16[1,2048,256]{2,1,0:T(8,128)(2,1)} %param.32) | copy-start | bytes 3145732
  110.4 2.8 %copy-start.1 = (bf16[1,2048,256]{2,1,0:T(8,128)(2,1)S(1)}, bf16[1,2048,256]{2,1,0:T(8,128)(2,1)}, u32[]{:S(2)}) copy-start(bf16[1,2048,256]{2,1,0:T(8,128)(2,1)} %param.33) | copy-start | bytes 3145732
  110.4 2.8 %copy-start.2 = (bf16[1,256,2048]{2,1,0:T(8,128)(2,1)S(1)}, bf16[1,256,2048]{2,1,0:T(8,128)(2,1)}, u32[]{:S(2)}) copy-start(bf16[1,256,2048]{2,1,0:T(8,128)(2,1)} %param.34) | copy-start | bytes 3145732
  110.6 2.6 %collective-permute-start.10 = (bf16[448,1024]{1,0:T(8,128)(2,1)S(1)}, bf16[448,1024]{1,0:T(8,128)(2,1)S(1)}, u32[]{:S(2)}, u32[]{:S(2)}) collective-permute-start(bf16[448,1024]{1,0:T(8,128)(2,1)S(1)} %bitcast.36), channel_id=1, source_target_pairs={{0,1},{1,0},{2,3},{3,2},{4,5},{5,4},{6,7},{7,6},{8,9},{9,8},{10,11... | collective-permute-start | bytes 2752520 | tf_op jit(solution)/shard_map/ppermute | solution.py:331
  110.7 4.5 %collective-permute-start.8 = (bf16[448,1024]{1,0:T(8,128)(2,1)S(1)}, bf16[448,1024]{1,0:T(8,128)(2,1)S(1)}, u32[]{:S(2)}, u32[]{:S(2)}) collective-permute-start(bf16[448,1024]{1,0:T(8,128)(2,1)S(1)} %bitcast.35), channel_id=1, source_target_pairs={{0,1},{1,0},{2,3},{3,2},{4,5},{5,4},{6,7},{7,6},{8,9},{9,8},{10,11... | collective-permute-start | bytes 2752520 | tf_op jit(solution)/shard_map/ppermute | solution.py:331
  115.0 2.6 %collective-permute-start.11 = (bf16[448,1024]{1,0:T(8,128)(2,1)S(1)}, bf16[448,1024]{1,0:T(8,128)(2,1)S(1)}, u32[]{:S(2)}, u32[]{:S(2)}) collective-permute-start(bf16[448,1024]{1,0:T(8,128)(2,1)S(1)} %get-tuple-element.46), channel_id=1, source_target_pairs={{0,1},{1,0},{2,3},{3,2},{4,5},{5,4},{6,7},{7,6},{8,9},{9,8},{10,11... | collective-permute-start | bytes 2752520 | tf_op jit(solution)/shard_map/ppermute | solution.py:331
  117.0 2.6 %collective-permute-start.9 = (bf16[448,1024]{1,0:T(8,128)(2,1)S(1)}, bf16[448,1024]{1,0:T(8,128)(2,1)S(1)}, u32[]{:S(2)}, u32[]{:S(2)}) collective-permute-start(bf16[448,1024]{1,0:T(8,128)(2,1)S(1)} %get-tuple-element.44), channel_id=1, source_target_pairs={{0,1},{1,0},{2,3},{3,2},{4,5},{5,4},{6,7},{7,6},{8,9},{9,8},{10,11... | collective-permute-start | bytes 2752520 | tf_op jit(solution)/shard_map/ppermute | solution.py:331
  161.0 13.3 %collective-permute-start.13 = (bf16[96,512]{1,0:T(8,128)(2,1)S(1)}, bf16[96,512]{1,0:T(8,128)(2,1)S(1)}, u32[]{:S(2)}, u32[]{:S(2)}) collective-permute-start(bf16[96,512]{1,0:T(8,128)(2,1)S(1)} %get-tuple-element.51), channel_id=1, source_target_pairs={{0,32},{1,33},{2,34},{3,35},{4,36},{5,37},{6,38},{7,39},{8,40},{9,... | collective-permute-start | bytes 294920 | tf_op jit(solution)/shard_map/ppermute | solution.py:328
  166.8 14.5 %collective-permute-start.15 = (bf16[96,512]{1,0:T(8,128)(2,1)S(1)}, bf16[96,512]{1,0:T(8,128)(2,1)S(1)}, u32[]{:S(2)}, u32[]{:S(2)}) collective-permute-start(bf16[96,512]{1,0:T(8,128)(2,1)S(1)} %get-tuple-element.53), channel_id=1, source_target_pairs={{0,96},{1,97},{2,98},{3,99},{4,100},{5,101},{6,102},{7,103},{8,104... | collective-permute-start | bytes 294920 | tf_op jit(solution)/shard_map/ppermute | solution.py:328
  169.5 16.9 %collective-permute-start.12 = (bf16[96,512]{1,0:T(8,128)(2,1)S(1)}, bf16[96,512]{1,0:T(8,128)(2,1)S(1)}, u32[]{:S(2)}, u32[]{:S(2)}) collective-permute-start(bf16[96,512]{1,0:T(8,128)(2,1)S(1)} %get-tuple-element.48), channel_id=1, source_target_pairs={{0,32},{1,33},{2,34},{3,35},{4,36},{5,37},{6,38},{7,39},{8,40},{9,... | collective-permute-start | bytes 294920 | tf_op jit(solution)/shard_map/ppermute | solution.py:328
  170.7 17.5 %collective-permute-start.17 = (bf16[96,512]{1,0:T(8,128)(2,1)S(1)}, bf16[96,512]{1,0:T(8,128)(2,1)S(1)}, u32[]{:S(2)}, u32[]{:S(2)}) collective-permute-start(bf16[96,512]{1,0:T(8,128)(2,1)S(1)} %get-tuple-element.54), channel_id=1, source_target_pairs={{0,96},{1,97},{2,98},{3,99},{4,100},{5,101},{6,102},{7,103},{8,104... | collective-permute-start | bytes 294920 | tf_op jit(solution)/shard_map/ppermute | solution.py:328
  174.4 16.9 %collective-permute-start.14 = (bf16[96,512]{1,0:T(8,128)(2,1)S(1)}, bf16[96,512]{1,0:T(8,128)(2,1)S(1)}, u32[]{:S(2)}, u32[]{:S(2)}) collective-permute-start(bf16[96,512]{1,0:T(8,128)(2,1)S(1)} %add_convert_fusion.3), channel_id=1, source_target_pairs={{0,96},{1,97},{2,98},{3,99},{4,100},{5,101},{6,102},{7,103},{8,104... | collective-permute-start | bytes 294920 | tf_op jit(solution)/shard_map/ppermute | solution.py:328
  181.3 14.2 %collective-permute-start.16 = (bf16[96,512]{1,0:T(8,128)(2,1)S(1)}, bf16[96,512]{1,0:T(8,128)(2,1)S(1)}, u32[]{:S(2)}, u32[]{:S(2)}) collective-permute-start(bf16[96,512]{1,0:T(8,128)(2,1)S(1)} %add_convert_fusion.2), channel_id=1, source_target_pairs={{0,32},{1,33},{2,34},{3,35},{4,36},{5,37},{6,38},{7,39},{8,40},{9,... | collective-permute-start | bytes 294920 | tf_op jit(solution)/shard_map/ppermute | solution.py:328

commit v2 on v1

--- a/solution.py
+++ b/solution.py
@@ -102,7 +102,7 @@
     rows, width = tokens.shape
     chans = w_in.shape[1]
     groups, entries = decay.shape
-    steps = 4
+    steps = 2
     c, g, s = chans // steps, groups // steps, groups * entries // steps
     return pl.pallas_call(
         mixer_kernel,
@@ -171,26 +171,48 @@
     )
 
 
-def block_kernel(first, spot, own, other, gate, up, down, keep, send):
+def halves(spot, half):
     core = spot[0] % 2
-    rows, half = other.shape
     here = pl.multiple_of(core * half, half)
     there = pl.multiple_of((1 - core) * half, half)
-    tile = rows // -(-rows // 256)
-    for i in range(0, rows, tile):
-        a, b = own[first + i : first + i + tile, :], other[i : i + tile, :]
-        gate_val = dot(a, gate[pl.ds(here, half), :]) + dot(b, gate[pl.ds(there, half), :])
-        up_val = dot(a, up[pl.ds(here, half), :]) + dot(b, up[pl.ds(there, half), :])
-        hidden = (jax.nn.silu(gate_val) * up_val).astype(bf16)
-        send[i : i + tile, :] = dot(hidden, down[:, pl.ds(there, half)]).astype(bf16)
-        keep[i : i + tile, :] = dot(hidden, down[:, pl.ds(here, half)]).astype(bf16)
-
-
-def block(spot, own, other, gate, up, down, first):
+    return pl.ds(here, half), pl.ds(there, half)
+
+
+def tiles(rows):
+    size = rows // -(-rows // 256)
+    return [slice(i, i + size) for i in range(0, rows, size)]
+
+
+def entry_kernel(spot, own, gate, up, part):
+    here, _ = halves(spot, own.shape[1])
+    hidden = gate.shape[1]
+    for rows in tiles(own.shape[0]):
+        part[rows, :hidden] = dot(own[rows, :], gate[here, :])
+        part[rows, hidden:] = dot(own[rows, :], up[here, :])
+
+
+def rest_kernel(first, spot, part, other, gate, up, down, keep, send):
+    here, there = halves(spot, other.shape[1])
+    hidden = gate.shape[1]
+    for rows in tiles(other.shape[0]):
+        done = slice(first + rows.start, first + rows.stop)
+        gate_val = part[done, :hidden] + dot(other[rows, :], gate[there, :])
+        up_val = part[done, hidden:] + dot(other[rows, :], up[there, :])
+        value = (jax.nn.silu(gate_val) * up_val).astype(bf16)
+        send[rows, :] = dot(value, down[:, there]).astype(bf16)
+        keep[rows, :] = dot(value, down[:, here]).astype(bf16)
+
+
+def entry(spot, own, gate, up):
+    shape = (own.shape[0], gate.shape[1] + up.shape[1])
+    return call(entry_kernel, spot, (own, gate, up), [(shape, f32)])[0]
+
+
+def rest(spot, part, other, gate, up, down, first):
     return call(
-        functools.partial(block_kernel, first),
+        functools.partial(rest_kernel, first),
         spot,
-        (own, other, gate, up, down),
+        (part, other, gate, up, down),
         [(other.shape, bf16)] * 2,
     )
 
@@ -377,7 +399,10 @@
     below_l, above_r = pair(own_l, 0), pair(own_r, 1)
     below_r, above_l = pair(own_r, 0), pair(own_l, 1)
     far_l, far_r = pair(below_l, 1), pair(above_r, 0)
-    shared_keep, shared_send = block(spot, own, other, shared_gate, shared_up, shared_down, 0)
+    shared_part = entry(spot, own, shared_gate, shared_up)
+    shared_keep, shared_send = rest(
+        spot, shared_part, other, shared_gate, shared_up, shared_down, 0
+    )
     shared_recv = swap(shared_send)
     sizes = (slot_cap, planes, slots)
     part, mix_near = call(
@@ -397,10 +422,13 @@
     )
 
     arrived = exchange(rows)
-    cut = total // 2
-    others = [swap(arrived[i : i + cut]) for i in (0, cut)]
+    cut = total * 4 // 7
     weights = (expert_gate[0], expert_up[0], expert_down[0])
-    outs = [block(spot, arrived, o, *weights, i) for o, i in zip(others, (0, cut))]
+    others = [swap(arrived[:cut]), swap(arrived[cut:])]
+    part = entry(spot, arrived, *weights[:2])
+    outs = []
+    for other, first in zip(others, (0, cut)):
+        outs.append(rest(spot, part, other, *weights, first))
     summed = [keep.astype(f32) + swap(send).astype(f32) for keep, send in outs]
     back = exchange(jnp.concatenate(summed, axis=0).astype(bf16))
 
@@ -414,9 +442,9 @@
     above_left = pair((m_above_l + in_l.astype(f32)).astype(bf16), 1)
     below_right = pair((m_below_r + in_r.astype(f32)).astype(bf16), 0)
     shared_out = shared_keep.astype(f32) + shared_recv.astype(f32)
-    rest = middle.astype(f32) + shared_out + m_own
-    left = rest[:, :half] + below_left.astype(f32) + above_left.astype(f32)
-    right = rest[:, half:] + below_right.astype(f32) + above_right.astype(f32)
+    known = middle.astype(f32) + shared_out + m_own
+    left = known[:, :half] + below_left.astype(f32) + above_left.astype(f32)
+    right = known[:, half:] + below_right.astype(f32) + above_right.astype(f32)
     layer_out = jnp.concatenate([left, right], axis=1).astype(bf16)
     return (layer_out, new_state)
 

time: 198 us -> 195 us (0.985)
  starting transfers between devices: 63.8 us -> 60.1 us
  waiting for transfers between devices: 24 us -> 26.8 us
  Pallas kernels: 17.6 us -> 15.4 us
    ppermute x12, starting transfers between devices: 62.1 us -> 58.1 us  [pair(): lax.ppermute(value, AXES, [(at(z, x, t), at(mate(z), x, t)) for z, x, t i...]
    ppermute x12, waiting for transfers between devices: 18.3 us -> 21.9 us  [pair(): lax.ppermute(value, AXES, [(at(z, x, t), at(mate(z), x, t)) for z, x, t i...]
    pallas_call x8 -> x10, Pallas kernels: 10.1 us -> 9.32 us  [call(): pl.pallas_call(kernel, in_specs=[SM] + [VM] * len(arrays), out_specs=[VM]...]
where the time goes in v2:
time: 195 us; the launch traced here: 194 us
  blocking collectives  88.5 us (45%)
  starting transfers between devices  60.1 us (31%)
  waiting for transfers between devices  26.8 us (14%)
  Pallas kernels  15.4 us (8%)
    all_to_all x2, blocking collectives, exchange(): lax.all_to_all(tiles, AXES, 0, 0, axis_index_groups=nearby, tiled=True)  88.5 us
    ppermute x12, starting transfers between devices, pair(): lax.ppermute(value, AXES, [(at(z, x, t), at(mate(z), x, t)) for z, x, t i...  58.1 us
    ppermute x12, waiting for transfers between devices, pair(): lax.ppermute(value, AXES, [(at(z, x, t), at(mate(z), x, t)) for z, x, t i...  21.9 us
    pallas_call x10, Pallas kernels, call(): pl.pallas_call(kernel, in_specs=[SM] + [VM] * len(arrays), out_specs=[VM]...  9.32 us
    pallas_call x1, Pallas kernels, mixer(): pl.pallas_call(mixer_kernel, grid=(steps,), in_specs=[VM, pl.BlockSpec((1...  6.12 us
    ppermute x6, waiting for transfers between devices, swap(): return lax.ppermute(value, 'tp', [(t, cores - 1 - t) for t in range(cores)])  4.92 us
  transfers between devices with their start and end apart: 18, of which 12 were waited for; matrix products, arithmetic and copies ran while one was open for 0% of the time, Pallas kernels for 4%

profile of v2, /device:TPU:34, one launch (start us, length us, event | category | flops | bytes accessed | tf_op | source)
XLA Modules:
  0.0 194.1 jit_solution(10660713085470446272)
XLA Ops:
  0.7 6.1 %mixer.1 = (f32[2,96,2048]{2,1,0:T(8,128)}, bf16[96,2048]{1,0:T(8,128)(2,1)S(1)}) custom-call(bf16[96,2048]{1,0:T(8,128)(2,1)} %tok.3, f32[1,2048]{1,0:T(1,128)} %bitcast.38, bf16[2048,512]{1,0:T(8,128)(2,1)} %w_in.1, f32[2,96,2048]{2,1,0:T(8,128)} %state.1, f32[32,64]{1,0:T(8,128)} %decay.1, f32[32,64]{1,0:T(8,128)} %freq.1, f32[1,32]{1,0:T(1,128)} %bitcast.40, ...), custom_call_target="tpu_custom_call" | custom-call | tf_op jit(solution)/shard_map/mixer/pallas_call | solution.py:107
  7.0 1.6 collective-permute-done.other
  9.0 10.7 %collective-permute-start.1 = (bf16[104,512]{1,0:T(8,128)(2,1)S(1)}, bf16[104,512]{1,0:T(8,128)(2,1)S(1)}, u32[]{:S(2)}, u32[]{:S(2)}) collective-permute-start(bf16[104,512]{1,0:T(8,128)(2,1)S(1)} %get-tuple-element.31.own_l), channel_id=1, source_target_pairs={{0,32},{1,33},{2,34},{3,35},{4,36},{5,37},{6,38},{7,39},{8,40},{9,... | collective-permute-start | bytes 319496 | tf_op jit(solution)/shard_map/ppermute | solution.py:350
  20.9 11.0 %collective-permute-start.4 = (bf16[96,512]{1,0:T(8,128)(2,1)S(1)}, bf16[96,512]{1,0:T(8,128)(2,1)S(1)}, u32[]{:S(2)}, u32[]{:S(2)}) collective-permute-start(bf16[96,512]{1,0:T(8,128)(2,1)S(1)} %get-tuple-element.32.own_r), channel_id=1, source_target_pairs={{0,96},{1,97},{2,98},{3,99},{4,100},{5,101},{6,102},{7,103},{8,104... | collective-permute-start | bytes 294920 | tf_op jit(solution)/shard_map/ppermute | solution.py:350
  32.0 7.5 %collective-permute-start.6 = (bf16[104,512]{1,0:T(8,128)(2,1)S(1)}, bf16[104,512]{1,0:T(8,128)(2,1)S(1)}, u32[]{:S(2)}, u32[]{:S(2)}) collective-permute-start(bf16[104,512]{1,0:T(8,128)(2,1)S(1)} %collective-permute-done.1.below_l), channel_id=1, source_target_pairs={{0,96},{1,97},{2,98},{3,99},{4,100},{5,101},{6,102},{7,103},{8,104... | collective-permute-start | bytes 319496 | tf_op jit(solution)/shard_map/ppermute | solution.py:350
  39.5 5.9 %collective-permute-start.2 = (bf16[96,512]{1,0:T(8,128)(2,1)S(1)}, bf16[96,512]{1,0:T(8,128)(2,1)S(1)}, u32[]{:S(2)}, u32[]{:S(2)}) collective-permute-start(bf16[96,512]{1,0:T(8,128)(2,1)S(1)} %get-tuple-element.32.own_r), channel_id=1, source_target_pairs={{0,32},{1,33},{2,34},{3,35},{4,36},{5,37},{6,38},{7,39},{8,40},{9,... | collective-permute-start | bytes 294920 | tf_op jit(solution)/shard_map/ppermute | solution.py:350
  45.5 5.7 %collective-permute-start.7 = (bf16[96,512]{1,0:T(8,128)(2,1)S(1)}, bf16[96,512]{1,0:T(8,128)(2,1)S(1)}, u32[]{:S(2)}, u32[]{:S(2)}) collective-permute-start(bf16[96,512]{1,0:T(8,128)(2,1)S(1)} %collective-permute-done.4.above_r), channel_id=1, source_target_pairs={{0,32},{1,33},{2,34},{3,35},{4,36},{5,37},{6,38},{7,39},{8,40},{9,... | collective-permute-start | bytes 294920 | tf_op jit(solution)/shard_map/ppermute | solution.py:350
  51.2 1.3 collective-permute-done.2.below_r
  52.4 2.5 %collective-permute-done.3.above_l = bf16[104,512]{1,0:T(8,128)(2,1)S(1)} collective-permute-done((bf16[104,512]{1,0:T(8,128)(2,1)S(1)}, bf16[104,512]{1,0:T(8,128)(2,1)S(1)}, u32[]{:S(2)}, u32[]{:S(2)}) %collective-permute-start.3) | collective-permute-done | bytes 106528 | tf_op jit(solution)/shard_map/ppermute | solution.py:350
  55.0 1.9 shard_map.204
  56.9 2.3 %collective-permute-done.7.far_r = bf16[96,512]{1,0:T(8,128)(2,1)S(1)} collective-permute-done((bf16[96,512]{1,0:T(8,128)(2,1)S(1)}, bf16[96,512]{1,0:T(8,128)(2,1)S(1)}, u32[]{:S(2)}, u32[]{:S(2)}) %collective-permute-start.7) | collective-permute-done | bytes 98336 | tf_op jit(solution)/shard_map/ppermute | solution.py:350
  59.2 0.8 shard_map.207
  60.0 48.5 %all_to_all.10 = bf16[16,56,1024]{2,1,0:T(8,128)(2,1)S(1)} all-to-all(bf16[16,56,1024]{2,1,0:T(8,128)(2,1)S(1)} %bitcast.33), channel_id=1, replica_groups={{0,2,4,6,8,10,12,14,16,18,20,22,24,26,28,30},{1,3,5,7,9,11,13,15,113,11..., dimensions={0} | all-to-all | bytes 3670016 | tf_op jit(solution)/shard_map/all_to_all | solution.py:367
  108.8 0.8 collective-permute-start.10
  110.0 1.1 shard_map.208.part
  111.2 1.3 collective-permute-done.10.other
  112.5 1.2 shard_map.210
  114.0 1.5 shard_map.209
  116.4 1.8 collective-permute-done.9
  118.8 40.0 %all_to_all.11 = bf16[16,56,1024]{2,1,0:T(8,128)(2,1)S(1)} all-to-all(bf16[16,56,1024]{2,1,0:T(8,128)(2,1)S(1)} %bitcast.35), channel_id=1, replica_groups={{0,2,4,6,8,10,12,14,16,18,20,22,24,26,28,30},{1,3,5,7,9,11,13,15,113,11..., dimensions={0} | all-to-all | bytes 3670016 | tf_op jit(solution)/shard_map/all_to_all | solution.py:367
  159.3 4.0 %collective-permute-start.13 = (bf16[96,512]{1,0:T(8,128)(2,1)S(1)}, bf16[96,512]{1,0:T(8,128)(2,1)S(1)}, u32[]{:S(2)}, u32[]{:S(2)}) collective-permute-start(bf16[96,512]{1,0:T(8,128)(2,1)S(1)} %get-tuple-element.51), channel_id=1, source_target_pairs={{0,32},{1,33},{2,34},{3,35},{4,36},{5,37},{6,38},{7,39},{8,40},{9,... | collective-permute-start | bytes 294920 | tf_op jit(solution)/shard_map/ppermute | solution.py:350
  163.2 1.1 shard_map.211
  164.3 3.1 %collective-permute-start.15 = (bf16[96,512]{1,0:T(8,128)(2,1)S(1)}, bf16[96,512]{1,0:T(8,128)(2,1)S(1)}, u32[]{:S(2)}, u32[]{:S(2)}) collective-permute-start(bf16[96,512]{1,0:T(8,128)(2,1)S(1)} %get-tuple-element.53), channel_id=1, source_target_pairs={{0,96},{1,97},{2,98},{3,99},{4,100},{5,101},{6,102},{7,103},{8,104... | collective-permute-start | bytes 294920 | tf_op jit(solution)/shard_map/ppermute | solution.py:350
  167.4 1.1 collective-permute-start.12
  168.6 3.9 %collective-permute-start.17 = (bf16[96,512]{1,0:T(8,128)(2,1)S(1)}, bf16[96,512]{1,0:T(8,128)(2,1)S(1)}, u32[]{:S(2)}, u32[]{:S(2)}) collective-permute-start(bf16[96,512]{1,0:T(8,128)(2,1)S(1)} %get-tuple-element.54), channel_id=1, source_target_pairs={{0,96},{1,97},{2,98},{3,99},{4,100},{5,101},{6,102},{7,103},{8,104... | collective-permute-start | bytes 294920 | tf_op jit(solution)/shard_map/ppermute | solution.py:350
  172.6 3.8 %collective-permute-start.14 = (bf16[96,512]{1,0:T(8,128)(2,1)S(1)}, bf16[96,512]{1,0:T(8,128)(2,1)S(1)}, u32[]{:S(2)}, u32[]{:S(2)}) collective-permute-start(bf16[96,512]{1,0:T(8,128)(2,1)S(1)} %add_convert_fusion.3), channel_id=1, source_target_pairs={{0,96},{1,97},{2,98},{3,99},{4,100},{5,101},{6,102},{7,103},{8,104... | collective-permute-start | bytes 294920 | tf_op jit(solution)/shard_map/ppermute | solution.py:350
  176.4 5.6 %collective-permute-done.15 = bf16[96,512]{1,0:T(8,128)(2,1)S(1)} collective-permute-done((bf16[96,512]{1,0:T(8,128)(2,1)S(1)}, bf16[96,512]{1,0:T(8,128)(2,1)S(1)}, u32[]{:S(2)}, u32[]{:S(2)}) %collective-permute-start.15) | collective-permute-done | bytes 98336 | tf_op jit(solution)/shard_map/ppermute | solution.py:350
  182.1 1.2 collective-permute-start.16
  183.4 2.8 %collective-permute-done.17 = bf16[96,512]{1,0:T(8,128)(2,1)S(1)} collective-permute-done((bf16[96,512]{1,0:T(8,128)(2,1)S(1)}, bf16[96,512]{1,0:T(8,128)(2,1)S(1)}, u32[]{:S(2)}, u32[]{:S(2)}) %collective-permute-start.17) | collective-permute-done | bytes 98336 | tf_op jit(solution)/shard_map/ppermute | solution.py:350
  186.2 3.4 %collective-permute-done.14 = bf16[96,512]{1,0:T(8,128)(2,1)S(1)} collective-permute-done((bf16[96,512]{1,0:T(8,128)(2,1)S(1)}, bf16[96,512]{1,0:T(8,128)(2,1)S(1)}, u32[]{:S(2)}, u32[]{:S(2)}) %collective-permute-start.14) | collective-permute-done | bytes 98336 | tf_op jit(solution)/shard_map/ppermute | solution.py:350
  189.6 3.7 %collective-permute-done.16 = bf16[96,512]{1,0:T(8,128)(2,1)S(1)} collective-permute-done((bf16[96,512]{1,0:T(8,128)(2,1)S(1)}, bf16[96,512]{1,0:T(8,128)(2,1)S(1)}, u32[]{:S(2)}, u32[]{:S(2)}) %collective-permute-start.16) | collective-permute-done | bytes 98336 | tf_op jit(solution)/shard_map/ppermute | solution.py:350
  193.4 0.7 pad_maximum_fusion.1
  (51 shorter events, 5.1 us)
Async XLA Ops:
  0.6 6.3 %copy-start.8 = (s32[96,6]{0,1:T(8,128)S(1)}, s32[96,6]{0,1:T(8,128)}, u32[]{:S(2)}) copy-start(s32[96,6]{0,1:T(8,128)} %param.38) | copy-start | bytes 6916
  0.6 6.3 %copy-start.9 = (f32[96,6]{0,1:T(8,128)S(1)}, f32[96,6]{0,1:T(8,128)}, u32[]{:S(2)}) copy-start(f32[96,6]{0,1:T(8,128)} %param.39) | copy-start | bytes 6916
  0.7 8.0 %copy-start.5 = (bf16[96,2048]{1,0:T(8,128)(2,1)S(1)}, bf16[96,2048]{1,0:T(8,128)(2,1)}, u32[]{:S(2)}) copy-start(bf16[96,2048]{1,0:T(8,128)(2,1)} %tok.3) | copy-start | bytes 1179652
  0.7 8.0 %copy-start.7 = (f32[2048]{0:T(1024)S(1)}, f32[2048]{0:T(1024)}, u32[]{:S(2)}) copy-start(f32[2048]{0:T(1024)} %param.31) | copy-start | bytes 24580
  0.7 19.1 %copy-start.3 = (bf16[2048,256]{1,0:T(8,128)(2,1)S(1)}, bf16[2048,256]{1,0:T(8,128)(2,1)}, u32[]{:S(2)}) copy-start(bf16[2048,256]{1,0:T(8,128)(2,1)} %up.3) | copy-start | bytes 3145732
  6.8 13.0 %copy-start.2 = (bf16[2048,256]{1,0:T(8,128)(2,1)S(1)}, bf16[2048,256]{1,0:T(8,128)(2,1)}, u32[]{:S(2)}) copy-start(bf16[2048,256]{1,0:T(8,128)(2,1)} %gate.3) | copy-start | bytes 3145732
  6.8 1.8 collective-permute-start
  8.7 11.4 %copy-start.6 = (bf16[256,2048]{1,0:T(8,128)(2,1)S(1)}, bf16[256,2048]{1,0:T(8,128)(2,1)}, u32[]{:S(2)}) copy-start(bf16[256,2048]{1,0:T(8,128)(2,1)} %down.1) | copy-start | bytes 3145732
  9.0 23.0 %collective-permute-start.1 = (bf16[104,512]{1,0:T(8,128)(2,1)S(1)}, bf16[104,512]{1,0:T(8,128)(2,1)S(1)}, u32[]{:S(2)}, u32[]{:S(2)}) collective-permute-start(bf16[104,512]{1,0:T(8,128)(2,1)S(1)} %get-tuple-element.31.own_l), channel_id=1, source_target_pairs={{0,32},{1,33},{2,34},{3,35},{4,36},{5,37},{6,38},{7,39},{8,40},{9,... | collective-permute-start | bytes 319496 | tf_op jit(solution)/shard_map/ppermute | solution.py:350
  20.7 36.2 %collective-permute-start.5 = (bf16[96,1024]{1,0:T(8,128)(2,1)S(1)}, bf16[96,1024]{1,0:T(8,128)(2,1)S(1)}, u32[]{:S(2)}, u32[]{:S(2)}) collective-permute-start(bf16[96,1024]{1,0:T(8,128)(2,1)S(1)} %get-tuple-element.37), channel_id=1, source_target_pairs={{0,1},{1,0},{2,3},{3,2},{4,5},{5,4},{6,7},{7,6},{8,9},{9,8},{10,11... | collective-permute-start | bytes 589832 | tf_op jit(solution)/shard_map/ppermute | solution.py:353
  20.9 24.6 %collective-permute-start.4 = (bf16[96,512]{1,0:T(8,128)(2,1)S(1)}, bf16[96,512]{1,0:T(8,128)(2,1)S(1)}, u32[]{:S(2)}, u32[]{:S(2)}) collective-permute-start(bf16[96,512]{1,0:T(8,128)(2,1)S(1)} %get-tuple-element.32.own_r), channel_id=1, source_target_pairs={{0,96},{1,97},{2,98},{3,99},{4,100},{5,101},{6,102},{7,103},{8,104... | collective-permute-start | bytes 294920 | tf_op jit(solution)/shard_map/ppermute | solution.py:350
  31.9 23.1 %collective-permute-start.3 = (bf16[104,512]{1,0:T(8,128)(2,1)S(1)}, bf16[104,512]{1,0:T(8,128)(2,1)S(1)}, u32[]{:S(2)}, u32[]{:S(2)}) collective-permute-start(bf16[104,512]{1,0:T(8,128)(2,1)S(1)} %get-tuple-element.31.own_l), channel_id=1, source_target_pairs={{0,96},{1,97},{2,98},{3,99},{4,100},{5,101},{6,102},{7,103},{8,104... | collective-permute-start | bytes 319496 | tf_op jit(solution)/shard_map/ppermute | solution.py:350
  32.0 27.2 %collective-permute-start.6 = (bf16[104,512]{1,0:T(8,128)(2,1)S(1)}, bf16[104,512]{1,0:T(8,128)(2,1)S(1)}, u32[]{:S(2)}, u32[]{:S(2)}) collective-permute-start(bf16[104,512]{1,0:T(8,128)(2,1)S(1)} %collective-permute-done.1.below_l), channel_id=1, source_target_pairs={{0,96},{1,97},{2,98},{3,99},{4,100},{5,101},{6,102},{7,103},{8,104... | collective-permute-start | bytes 319496 | tf_op jit(solution)/shard_map/ppermute | solution.py:350
  39.5 12.9 %collective-permute-start.2 = (bf16[96,512]{1,0:T(8,128)(2,1)S(1)}, bf16[96,512]{1,0:T(8,128)(2,1)S(1)}, u32[]{:S(2)}, u32[]{:S(2)}) collective-permute-start(bf16[96,512]{1,0:T(8,128)(2,1)S(1)} %get-tuple-element.32.own_r), channel_id=1, source_target_pairs={{0,32},{1,33},{2,34},{3,35},{4,36},{5,37},{6,38},{7,39},{8,40},{9,... | collective-permute-start | bytes 294920 | tf_op jit(solution)/shard_map/ppermute | solution.py:350
  45.5 13.7 %collective-permute-start.7 = (bf16[96,512]{1,0:T(8,128)(2,1)S(1)}, bf16[96,512]{1,0:T(8,128)(2,1)S(1)}, u32[]{:S(2)}, u32[]{:S(2)}) collective-permute-start(bf16[96,512]{1,0:T(8,128)(2,1)S(1)} %collective-permute-done.4.above_r), channel_id=1, source_target_pairs={{0,32},{1,33},{2,34},{3,35},{4,36},{5,37},{6,38},{7,39},{8,40},{9,... | collective-permute-start | bytes 294920 | tf_op jit(solution)/shard_map/ppermute | solution.py:350
  108.5 1.2 copy-start
  108.5 1.5 copy-start.1
  108.6 5.4 %collective-permute-start.8 = (bf16[512,1024]{1,0:T(8,128)(2,1)S(1)}, bf16[512,1024]{1,0:T(8,128)(2,1)S(1)}, u32[]{:S(2)}, u32[]{:S(2)}) collective-permute-start(bf16[512,1024]{1,0:T(8,128)(2,1)S(1)} %slice.16), channel_id=1, source_target_pairs={{0,1},{1,0},{2,3},{3,2},{4,5},{5,4},{6,7},{7,6},{8,9},{9,8},{10,11... | collective-permute-start | bytes 3145736 | tf_op jit(solution)/shard_map/ppermute | solution.py:353
  108.8 3.7 %collective-permute-start.10 = (bf16[384,1024]{1,0:T(8,128)(2,1)S(1)}, bf16[384,1024]{1,0:T(8,128)(2,1)S(1)}, u32[]{:S(2)}, u32[]{:S(2)}) collective-permute-start(bf16[384,1024]{1,0:T(8,128)(2,1)S(1)} %slice.17), channel_id=1, source_target_pairs={{0,1},{1,0},{2,3},{3,2},{4,5},{5,4},{6,7},{7,6},{8,9},{9,8},{10,11... | collective-permute-start | bytes 2359304 | tf_op jit(solution)/shard_map/ppermute | solution.py:353
  110.0 2.4 %copy-start.4 = (bf16[1,256,2048]{2,1,0:T(8,128)(2,1)S(1)}, bf16[1,256,2048]{2,1,0:T(8,128)(2,1)}, u32[]{:S(2)}) copy-start(bf16[1,256,2048]{2,1,0:T(8,128)(2,1)} %param.34) | copy-start | bytes 3145732
  113.7 2.4 %collective-permute-start.11 = (bf16[384,1024]{1,0:T(8,128)(2,1)S(1)}, bf16[384,1024]{1,0:T(8,128)(2,1)S(1)}, u32[]{:S(2)}, u32[]{:S(2)}) collective-permute-start(bf16[384,1024]{1,0:T(8,128)(2,1)S(1)} %get-tuple-element.46), channel_id=1, source_target_pairs={{0,1},{1,0},{2,3},{3,2},{4,5},{5,4},{6,7},{7,6},{8,9},{9,8},{10,11... | collective-permute-start | bytes 2359304 | tf_op jit(solution)/shard_map/ppermute | solution.py:353
  115.4 2.8 %collective-permute-start.9 = (bf16[512,1024]{1,0:T(8,128)(2,1)S(1)}, bf16[512,1024]{1,0:T(8,128)(2,1)S(1)}, u32[]{:S(2)}, u32[]{:S(2)}) collective-permute-start(bf16[512,1024]{1,0:T(8,128)(2,1)S(1)} %get-tuple-element.44), channel_id=1, source_target_pairs={{0,1},{1,0},{2,3},{3,2},{4,5},{5,4},{6,7},{7,6},{8,9},{9,8},{10,11... | collective-permute-start | bytes 3145736 | tf_op jit(solution)/shard_map/ppermute | solution.py:353
  159.3 13.3 %collective-permute-start.13 = (bf16[96,512]{1,0:T(8,128)(2,1)S(1)}, bf16[96,512]{1,0:T(8,128)(2,1)S(1)}, u32[]{:S(2)}, u32[]{:S(2)}) collective-permute-start(bf16[96,512]{1,0:T(8,128)(2,1)S(1)} %get-tuple-element.51), channel_id=1, source_target_pairs={{0,32},{1,33},{2,34},{3,35},{4,36},{5,37},{6,38},{7,39},{8,40},{9,... | collective-permute-start | bytes 294920 | tf_op jit(solution)/shard_map/ppermute | solution.py:350
  164.3 17.7 %collective-permute-start.15 = (bf16[96,512]{1,0:T(8,128)(2,1)S(1)}, bf16[96,512]{1,0:T(8,128)(2,1)S(1)}, u32[]{:S(2)}, u32[]{:S(2)}) collective-permute-start(bf16[96,512]{1,0:T(8,128)(2,1)S(1)} %get-tuple-element.53), channel_id=1, source_target_pairs={{0,96},{1,97},{2,98},{3,99},{4,100},{5,101},{6,102},{7,103},{8,104... | collective-permute-start | bytes 294920 | tf_op jit(solution)/shard_map/ppermute | solution.py:350
  167.4 15.9 %collective-permute-start.12 = (bf16[96,512]{1,0:T(8,128)(2,1)S(1)}, bf16[96,512]{1,0:T(8,128)(2,1)S(1)}, u32[]{:S(2)}, u32[]{:S(2)}) collective-permute-start(bf16[96,512]{1,0:T(8,128)(2,1)S(1)} %get-tuple-element.48), channel_id=1, source_target_pairs={{0,32},{1,33},{2,34},{3,35},{4,36},{5,37},{6,38},{7,39},{8,40},{9,... | collective-permute-start | bytes 294920 | tf_op jit(solution)/shard_map/ppermute | solution.py:350
  168.6 17.7 %collective-permute-start.17 = (bf16[96,512]{1,0:T(8,128)(2,1)S(1)}, bf16[96,512]{1,0:T(8,128)(2,1)S(1)}, u32[]{:S(2)}, u32[]{:S(2)}) collective-permute-start(bf16[96,512]{1,0:T(8,128)(2,1)S(1)} %get-tuple-element.54), channel_id=1, source_target_pairs={{0,96},{1,97},{2,98},{3,99},{4,100},{5,101},{6,102},{7,103},{8,104... | collective-permute-start | bytes 294920 | tf_op jit(solution)/shard_map/ppermute | solution.py:350
  172.6 17.0 %collective-permute-start.14 = (bf16[96,512]{1,0:T(8,128)(2,1)S(1)}, bf16[96,512]{1,0:T(8,128)(2,1)S(1)}, u32[]{:S(2)}, u32[]{:S(2)}) collective-permute-start(bf16[96,512]{1,0:T(8,128)(2,1)S(1)} %add_convert_fusion.3), channel_id=1, source_target_pairs={{0,96},{1,97},{2,98},{3,99},{4,100},{5,101},{6,102},{7,103},{8,104... | collective-permute-start | bytes 294920 | tf_op jit(solution)/shard_map/ppermute | solution.py:350
  182.1 11.3 %collective-permute-start.16 = (bf16[96,512]{1,0:T(8,128)(2,1)S(1)}, bf16[96,512]{1,0:T(8,128)(2,1)S(1)}, u32[]{:S(2)}, u32[]{:S(2)}) collective-permute-start(bf16[96,512]{1,0:T(8,128)(2,1)S(1)} %add_convert_fusion.2), channel_id=1, source_target_pairs={{0,32},{1,33},{2,34},{3,35},{4,36},{5,37},{6,38},{7,39},{8,40},{9,... | collective-permute-start | bytes 294920 | tf_op jit(solution)/shard_map/ppermute | solution.py:350

commit v3 on v2

--- a/solution.py
+++ b/solution.py
@@ -140,7 +140,7 @@
 
 
 def second_norm_kernel(
-    spot, tok, mine, other, gain, table, own_half, far_half, mid_half, left, right, normed, mid
+    spot, tok, mine, other, gain, table, own_half, far_half, mid_half, travel, normed, mid
 ):
     core = spot[0] % 2
     rows, half = far_half.shape
@@ -151,9 +151,8 @@
     there = pl.multiple_of((1 - core) * half, half)
     own = normed[:, pl.ds(here, half)]
     own_half[...] = own
-    left[:rows, :] = own[:, : half // 2]
-    left[rows:, :] = table[...]
-    right[...] = own[:, half // 2 :]
+    travel[:rows, :] = own
+    travel[rows:, :] = table[...]
     far_half[...] = normed[:, pl.ds(there, half)]
     mid_half[...] = mid[:, pl.ds(here, half)]
 
@@ -166,7 +165,7 @@
         spot,
         (tokens, mine, other, gain, table),
         [((rows, half), bf16)] * 3
-        + [((rows + TABLE, half // 2), bf16), ((rows, half // 2), bf16)],
+        + [((rows + TABLE, half), bf16)],
         [pltpu.VMEM((rows, width), bf16), pltpu.VMEM((rows, width), bf16)],
     )
 
@@ -241,7 +240,9 @@
     rank = dot(hits.astype(bf16), before)
     home = plane // NEAR
     clusters = planes // NEAR
-    home = (home, home + 1 - 2 * (home % 2), (home + clusters // 2) % clusters, clusters - 1 - home)[m]
+    even, odd = home + 1 - 2 * (home % 2), clusters - 1 - home
+    first, second = jnp.where(core == 0, even, odd), jnp.where(core == 0, odd, even)
+    home = (home, first, (home + clusters // 2) % clusters, second)[m]
     place = jnp.where(hits > 0.5, rank + (home * cap).astype(f32), -1.0)
     for d in range(0, dests, 2):
         ones = [(level == place[e : e + 1, :]).astype(f32) for e in (d, d + 1)]
@@ -255,53 +256,38 @@
     return ref[rows:, : 2 * LANES].astype(f32)
 
 
-def relay_near_kernel(
-    cap, planes, slots, spot, own_l, own_r, below_l, below_r, above_l, above_r, part, mix, pick
-):
+def relay_near_kernel(cap, planes, slots, spot, own, below, above, part, mix, pick):
     rows = pick.shape[2]
-    half = own_r.shape[1]
-    for i, (m, ref) in enumerate(((0, own_l), (1, below_l), (3, above_l))):
+    sources = (own, below, above)
+    for i, (m, ref) in enumerate(zip((0, 1, 3), sources)):
         slots_of(spot, cap, planes, slots, m, table_of(ref, rows), pick.at[i], mix.at[i])
     tile = 2 * slots
     for i in range(0, part.shape[0], tile):
         span = pl.ds(i, tile)
-        for at, refs in (
-            (slice(0, half), (own_l, below_l, above_l)),
-            (slice(half, None), (own_r, below_r, above_r)),
-        ):
-            sums = [dot(pick[n, span, :], ref[:rows, :]) for n, ref in enumerate(refs)]
-            part[span, at] = (sums[0] + sums[1] + sums[2]).astype(bf16)
-
-
-def relay_far_kernel(cap, planes, slots, spot, far_l, far_r, part, out, mix, pick):
+        sums = [dot(pick[n, span, :], ref[:rows, :]) for n, ref in enumerate(sources)]
+        part[span, :] = (sums[0] + sums[1] + sums[2]).astype(bf16)
+
+
+def relay_far_kernel(cap, planes, slots, spot, far, part, out, mix, pick):
     rows = pick.shape[1]
-    half = far_r.shape[1]
-    slots_of(spot, cap, planes, slots, 2, table_of(far_l, rows), pick, mix)
+    slots_of(spot, cap, planes, slots, 2, table_of(far, rows), pick, mix)
     tile = 2 * slots
     for i in range(0, part.shape[0], tile):
         span = pl.ds(i, tile)
-        one = pick[span, :]
-        out[span, :half] = part[span, :half] + dot(one, far_l[:rows, :]).astype(bf16)
-        out[span, half:] = part[span, half:] + dot(one, far_r[...]).astype(bf16)
+        out[span, :] = part[span, :] + dot(pick[span, :], far[:rows, :]).astype(bf16)
 
 
 TN = (((0,), (0,)), ((), ()))
 
 
-def mix_far_kernel(spot, mix, back, left, right):
-    half = left.shape[1]
-    far = lax.dot_general(mix[...], back[...], TN, preferred_element_type=f32).astype(bf16)
-    left[...] = far[:, :half]
-    right[...] = far[:, half:]
-
-
-def mix_near_kernel(spot, mix, back, own, below_l, below_r, above_l, above_r):
-    half = below_l.shape[1]
-    for i, (left, right) in ((1, (below_l, below_r)), (2, (above_l, above_r))):
+def mix_far_kernel(spot, mix, back, far):
+    far[...] = lax.dot_general(mix[...], back[...], TN, preferred_element_type=f32).astype(bf16)
+
+
+def mix_near_kernel(spot, mix, back, own, below, above):
+    for i, ref in ((1, below), (2, above), (0, own)):
         sums = lax.dot_general(mix[i], back[...], TN, preferred_element_type=f32)
-        left[...] = sums[:, :half].astype(left.dtype)
-        right[...] = sums[:, half:].astype(right.dtype)
-    own[...] = lax.dot_general(mix[0], back[...], TN, preferred_element_type=f32)
+        ref[...] = sums.astype(ref.dtype)
 
 
 def body(
@@ -335,7 +321,6 @@
     total = NEAR * RING * slots
     width = tokens.shape[1]
     wide = width // 2
-    half = wide // 2
 
     def at(z, x, t):
         return ((z % planes) * RING + x) * cores + t
@@ -343,11 +328,13 @@
     everyone = [(z, x, t) for z in range(planes) for x in range(RING) for t in range(cores)]
 
     def pair(value, shift):
-        def mate(z):
-            up = (z // NEAR + shift) % 2 == 0
+        def mate(z, t):
+            up = (z // NEAR + shift + t) % 2 == 0
             return z + NEAR if up else z - NEAR
 
-        return lax.ppermute(value, AXES, [(at(z, x, t), at(mate(z), x, t)) for z, x, t in everyone])
+        return lax.ppermute(
+            value, AXES, [(at(z, x, t), at(mate(z, t), x, t)) for z, x, t in everyone]
+        )
 
     def swap(value):
         return lax.ppermute(value, "tp", [(t, cores - 1 - t) for t in range(cores)])
@@ -374,7 +361,7 @@
         ],
         axis=1,
     )
-    table = jnp.pad(table, ((0, 0), (0, half - 2 * LANES)))
+    table = jnp.pad(table, ((0, 0), (0, wide - 2 * LANES)))
 
     lanes = input_map.shape[2]
     imap = input_map.transpose(0, 1, 3, 2).reshape(2, -1, lanes)
@@ -392,13 +379,12 @@
         skip_gain[None],
         out_weight,
     )
-    own, other, middle, own_l, own_r = second_norm(
+    own, other, middle, travel = second_norm(
         spot, tokens, partial, swap(partial), channel_gain[None], table
     )
 
-    below_l, above_r = pair(own_l, 0), pair(own_r, 1)
-    below_r, above_l = pair(own_r, 0), pair(own_l, 1)
-    far_l, far_r = pair(below_l, 1), pair(above_r, 0)
+    below, above = pair(travel, 0), pair(travel, 1)
+    far = pair(below, 1)
     shared_part = entry(spot, own, shared_gate, shared_up)
     shared_keep, shared_send = rest(
         spot, shared_part, other, shared_gate, shared_up, shared_down, 0
@@ -408,7 +394,7 @@
     part, mix_near = call(
         functools.partial(relay_near_kernel, *sizes),
         spot,
-        (own_l, own_r, below_l, below_r, above_l, above_r),
+        (travel, below, above),
         [((total, wide), bf16), ((3, total, seq_rows), bf16)],
         [pltpu.VMEM((3, total, seq_rows), bf16)],
     )
@@ -416,7 +402,7 @@
     rows, mix_far = call(
         functools.partial(relay_far_kernel, *sizes),
         spot,
-        (far_l, far_r, part),
+        (far, part),
         [((total, wide), bf16), ((total, seq_rows), bf16)],
         [pltpu.VMEM((total, seq_rows), bf16)],
     )
@@ -432,20 +418,15 @@
     summed = [keep.astype(f32) + swap(send).astype(f32) for keep, send in outs]
     back = exchange(jnp.concatenate(summed, axis=0).astype(bf16))
 
-    sent, sums = ((seq_rows, half), bf16), ((seq_rows, half), f32)
-    m_far_l, m_far_r = call(mix_far_kernel, spot, (mix_far, back), [sent] * 2)
-    in_l, in_r = pair(m_far_l, 0), pair(m_far_r, 1)
-    m_own, m_below_l, m_below_r, m_above_l, m_above_r = call(
-        mix_near_kernel, spot, (mix_near, back), [((seq_rows, wide), f32), sent, sums, sums, sent]
-    )
-    above_right, below_left = pair(m_above_r, 1), pair(m_below_l, 0)
-    above_left = pair((m_above_l + in_l.astype(f32)).astype(bf16), 1)
-    below_right = pair((m_below_r + in_r.astype(f32)).astype(bf16), 0)
+    sent, sums = ((seq_rows, wide), bf16), ((seq_rows, wide), f32)
+    m_far = call(mix_far_kernel, spot, (mix_far, back), [sent])[0]
+    passing = pair(m_far, 0)
+    m_own, m_below, m_above = call(mix_near_kernel, spot, (mix_near, back), [sums, sent, sums])
+    direct = pair(m_below, 0)
+    joined = pair((m_above + passing.astype(f32)).astype(bf16), 1)
     shared_out = shared_keep.astype(f32) + shared_recv.astype(f32)
     known = middle.astype(f32) + shared_out + m_own
-    left = known[:, :half] + below_left.astype(f32) + above_left.astype(f32)
-    right = known[:, half:] + below_right.astype(f32) + above_right.astype(f32)
-    layer_out = jnp.concatenate([left, right], axis=1).astype(bf16)
+    layer_out = (known + direct.astype(f32) + joined.astype(f32)).astype(bf16)
     return (layer_out, new_state)
 
 

time: 195 us -> 191 us (0.979)
  starting transfers between devices: 60.1 us -> 52.1 us
  waiting for transfers between devices: 26.8 us -> 30.4 us
    ppermute x12 -> x6, starting transfers between devices: 58.1 us -> 50.1 us  [pair(): lax.ppermute(value, AXES, [(at(z, x, t), at(mate(z, t), x, t)) for z, x,...]
    ppermute x12 -> x6, waiting for transfers between devices: 21.9 us -> 25.5 us  [pair(): lax.ppermute(value, AXES, [(at(z, x, t), at(mate(z, t), x, t)) for z, x,...]
  transfers between devices with their start and end apart: 18 -> 12, of which waited for: 12 -> 8; matrix products, arithmetic and copies ran while one was open for 0% -> 0% of each run, Pallas kernels for 4% -> 4%
where the time goes in v3:
time: 191 us; the launch traced here: 190 us
  blocking collectives  88.2 us (46%)
  starting transfers between devices  52.1 us (27%)
  waiting for transfers between devices  30.4 us (16%)
  Pallas kernels  15.4 us (8%)
    all_to_all x2, blocking collectives, exchange(): lax.all_to_all(tiles, AXES, 0, 0, axis_index_groups=nearby, tiled=True)  88.2 us
    ppermute x6, starting transfers between devices, pair(): lax.ppermute(value, AXES, [(at(z, x, t), at(mate(z, t), x, t)) for z, x,...  50.1 us
    ppermute x6, waiting for transfers between devices, pair(): lax.ppermute(value, AXES, [(at(z, x, t), at(mate(z, t), x, t)) for z, x,...  25.5 us
    pallas_call x10, Pallas kernels, call(): pl.pallas_call(kernel, in_specs=[SM] + [VM] * len(arrays), out_specs=[VM]...  9.26 us
    pallas_call x1, Pallas kernels, mixer(): pl.pallas_call(mixer_kernel, grid=(steps,), in_specs=[VM, pl.BlockSpec((1...  6.12 us
    ppermute x6, waiting for transfers between devices, swap(): return lax.ppermute(value, 'tp', [(t, cores - 1 - t) for t in range(cores)])  4.94 us
  transfers between devices with their start and end apart: 12, of which 8 were waited for; matrix products, arithmetic and copies ran while one was open for 0% of the time, Pallas kernels for 4%

profile of v3, /device:TPU:34, one launch (start us, length us, event | category | flops | bytes accessed | tf_op | source)
XLA Modules:
  0.0 189.6 jit_solution(17585329064598631181)
XLA Ops:
  0.7 6.1 %mixer.1 = (f32[2,96,2048]{2,1,0:T(8,128)}, bf16[96,2048]{1,0:T(8,128)(2,1)S(1)}) custom-call(bf16[96,2048]{1,0:T(8,128)(2,1)} %tok.3, f32[1,2048]{1,0:T(1,128)} %bitcast.38, bf16[2048,512]{1,0:T(8,128)(2,1)} %w_in.1, f32[2,96,2048]{2,1,0:T(8,128)} %state.1, f32[32,64]{1,0:T(8,128)} %decay.1, f32[32,64]{1,0:T(8,128)} %freq.1, f32[1,32]{1,0:T(1,128)} %bitcast.40, ...), custom_call_target="tpu_custom_call" | custom-call | tf_op jit(solution)/shard_map/mixer/pallas_call | solution.py:107
  7.0 1.6 collective-permute-done.other
  8.7 0.4 shard_map.203
  9.0 10.7 %collective-permute-start.1 = (bf16[104,1024]{1,0:T(8,128)(2,1)S(1)}, bf16[104,1024]{1,0:T(8,128)(2,1)S(1)}, u32[]{:S(2)}, u32[]{:S(2)}) collective-permute-start(bf16[104,1024]{1,0:T(8,128)(2,1)S(1)} %get-tuple-element.26.own), channel_id=1, source_target_pairs={{0,32},{1,97},{2,34},{3,99},{4,36},{5,101},{6,38},{7,103},{8,40},{... | collective-permute-start | bytes 638984 | tf_op jit(solution)/shard_map/ppermute | solution.py:335
  19.8 10.7 %collective-permute-start.2 = (bf16[104,1024]{1,0:T(8,128)(2,1)S(1)}, bf16[104,1024]{1,0:T(8,128)(2,1)S(1)}, u32[]{:S(2)}, u32[]{:S(2)}) collective-permute-start(bf16[104,1024]{1,0:T(8,128)(2,1)S(1)} %get-tuple-element.26.own), channel_id=1, source_target_pairs={{0,96},{1,33},{2,98},{3,35},{4,100},{5,37},{6,102},{7,39},{8,104},... | collective-permute-start | bytes 638984 | tf_op jit(solution)/shard_map/ppermute | solution.py:335
  30.5 22.4 %collective-permute-start.4 = (bf16[104,1024]{1,0:T(8,128)(2,1)S(1)}, bf16[104,1024]{1,0:T(8,128)(2,1)S(1)}, u32[]{:S(2)}, u32[]{:S(2)}) collective-permute-start(bf16[104,1024]{1,0:T(8,128)(2,1)S(1)} %collective-permute-done.1.below), channel_id=1, source_target_pairs={{0,96},{1,33},{2,98},{3,35},{4,100},{5,37},{6,102},{7,39},{8,104},... | collective-permute-start | bytes 638984 | tf_op jit(solution)/shard_map/ppermute | solution.py:335
  52.9 0.3 shard_map.205.part
  53.2 0.6 shard_map.206
  53.9 1.8 shard_map.204
  55.8 1.6 collective-permute-done.4.far
  57.4 0.8 shard_map.207
  58.2 49.4 %all_to_all.10 = bf16[16,56,1024]{2,1,0:T(8,128)(2,1)S(1)} all-to-all(bf16[16,56,1024]{2,1,0:T(8,128)(2,1)S(1)} %bitcast.33), channel_id=1, replica_groups={{0,2,4,6,8,10,12,14,16,18,20,22,24,26,28,30},{1,3,5,7,9,11,13,15,113,11..., dimensions={0} | all-to-all | bytes 3670016 | tf_op jit(solution)/shard_map/all_to_all | solution.py:354
  107.9 0.6 collective-permute-start.7
  108.5 0.3 copy-done
  108.8 0.3 copy-done.1
  109.1 1.1 shard_map.208.part
  110.2 1.3 collective-permute-done.7.other
  111.6 1.2 shard_map.210
  112.8 0.4 collective-permute-start.8
  113.2 1.5 shard_map.209
  114.7 0.5 collective-permute-start.6
  115.4 0.3 add_convert_fusion.1
  115.7 1.8 collective-permute-done.6
  117.5 0.4 add_convert_fusion
  118.0 38.8 %all_to_all.11 = bf16[16,56,1024]{2,1,0:T(8,128)(2,1)S(1)} all-to-all(bf16[16,56,1024]{2,1,0:T(8,128)(2,1)S(1)} %bitcast.35), channel_id=1, replica_groups={{0,2,4,6,8,10,12,14,16,18,20,22,24,26,28,30},{1,3,5,7,9,11,13,15,113,11..., dimensions={0} | all-to-all | bytes 3670016 | tf_op jit(solution)/shard_map/all_to_all | solution.py:354
  156.8 0.5 shard_map.212
  157.5 1.1 shard_map.211
  158.6 6.0 %collective-permute-start.9 = (bf16[96,1024]{1,0:T(8,128)(2,1)S(1)}, bf16[96,1024]{1,0:T(8,128)(2,1)S(1)}, u32[]{:S(2)}, u32[]{:S(2)}) collective-permute-start(bf16[96,1024]{1,0:T(8,128)(2,1)S(1)} %get-tuple-element.42), channel_id=1, source_target_pairs={{0,32},{1,97},{2,34},{3,99},{4,36},{5,101},{6,38},{7,103},{8,40},{... | collective-permute-start | bytes 589832 | tf_op jit(solution)/shard_map/ppermute | solution.py:335
  164.6 13.1 %collective-permute-done.10 = bf16[96,1024]{1,0:T(8,128)(2,1)S(1)} collective-permute-done((bf16[96,1024]{1,0:T(8,128)(2,1)S(1)}, bf16[96,1024]{1,0:T(8,128)(2,1)S(1)}, u32[]{:S(2)}, u32[]{:S(2)}) %collective-permute-start.10) | collective-permute-done | bytes 196640 | tf_op jit(solution)/shard_map/ppermute | solution.py:335
  177.9 2.1 %collective-permute-done.9 = bf16[96,1024]{1,0:T(8,128)(2,1)S(1)} collective-permute-done((bf16[96,1024]{1,0:T(8,128)(2,1)S(1)}, bf16[96,1024]{1,0:T(8,128)(2,1)S(1)}, u32[]{:S(2)}, u32[]{:S(2)}) %collective-permute-start.9) | collective-permute-done | bytes 196640 | tf_op jit(solution)/shard_map/ppermute | solution.py:335
  180.0 8.7 %collective-permute-done.11 = bf16[96,1024]{1,0:T(8,128)(2,1)S(1)} collective-permute-done((bf16[96,1024]{1,0:T(8,128)(2,1)S(1)}, bf16[96,1024]{1,0:T(8,128)(2,1)S(1)}, u32[]{:S(2)}, u32[]{:S(2)}) %collective-permute-start.11) | collective-permute-done | bytes 196640 | tf_op jit(solution)/shard_map/ppermute | solution.py:335
  188.7 0.9 add_convert_fusion.2
  (36 shorter events, 1.3 us)
Async XLA Ops:
  0.6 6.3 %copy-start.8 = (s32[96,6]{0,1:T(8,128)S(1)}, s32[96,6]{0,1:T(8,128)}, u32[]{:S(2)}) copy-start(s32[96,6]{0,1:T(8,128)} %param.38) | copy-start | bytes 6916
  0.6 6.3 %copy-start.9 = (f32[96,6]{0,1:T(8,128)S(1)}, f32[96,6]{0,1:T(8,128)}, u32[]{:S(2)}) copy-start(f32[96,6]{0,1:T(8,128)} %param.39) | copy-start | bytes 6916
  0.7 8.0 %copy-start.5 = (bf16[96,2048]{1,0:T(8,128)(2,1)S(1)}, bf16[96,2048]{1,0:T(8,128)(2,1)}, u32[]{:S(2)}) copy-start(bf16[96,2048]{1,0:T(8,128)(2,1)} %tok.3) | copy-start | bytes 1179652
  0.7 8.0 %copy-start.7 = (f32[2048]{0:T(1024)S(1)}, f32[2048]{0:T(1024)}, u32[]{:S(2)}) copy-start(f32[2048]{0:T(1024)} %param.31) | copy-start | bytes 24580
  0.7 52.2 %copy-start.3 = (bf16[2048,256]{1,0:T(8,128)(2,1)S(1)}, bf16[2048,256]{1,0:T(8,128)(2,1)}, u32[]{:S(2)}) copy-start(bf16[2048,256]{1,0:T(8,128)(2,1)} %up.3) | copy-start | bytes 3145732
  6.8 46.1 %copy-start.2 = (bf16[2048,256]{1,0:T(8,128)(2,1)S(1)}, bf16[2048,256]{1,0:T(8,128)(2,1)}, u32[]{:S(2)}) copy-start(bf16[2048,256]{1,0:T(8,128)(2,1)} %gate.3) | copy-start | bytes 3145732
  6.8 1.8 collective-permute-start
  8.7 44.5 %copy-start.6 = (bf16[256,2048]{1,0:T(8,128)(2,1)S(1)}, bf16[256,2048]{1,0:T(8,128)(2,1)}, u32[]{:S(2)}) copy-start(bf16[256,2048]{1,0:T(8,128)(2,1)} %down.1) | copy-start | bytes 3145732
  9.0 21.4 %collective-permute-start.1 = (bf16[104,1024]{1,0:T(8,128)(2,1)S(1)}, bf16[104,1024]{1,0:T(8,128)(2,1)S(1)}, u32[]{:S(2)}, u32[]{:S(2)}) collective-permute-start(bf16[104,1024]{1,0:T(8,128)(2,1)S(1)} %get-tuple-element.26.own), channel_id=1, source_target_pairs={{0,32},{1,97},{2,34},{3,99},{4,36},{5,101},{6,38},{7,103},{8,40},{... | collective-permute-start | bytes 638984 | tf_op jit(solution)/shard_map/ppermute | solution.py:335
  19.8 34.1 %collective-permute-start.2 = (bf16[104,1024]{1,0:T(8,128)(2,1)S(1)}, bf16[104,1024]{1,0:T(8,128)(2,1)S(1)}, u32[]{:S(2)}, u32[]{:S(2)}) collective-permute-start(bf16[104,1024]{1,0:T(8,128)(2,1)S(1)} %get-tuple-element.26.own), channel_id=1, source_target_pairs={{0,96},{1,33},{2,98},{3,35},{4,100},{5,37},{6,102},{7,39},{8,104},... | collective-permute-start | bytes 638984 | tf_op jit(solution)/shard_map/ppermute | solution.py:335
  30.5 26.9 %collective-permute-start.4 = (bf16[104,1024]{1,0:T(8,128)(2,1)S(1)}, bf16[104,1024]{1,0:T(8,128)(2,1)S(1)}, u32[]{:S(2)}, u32[]{:S(2)}) collective-permute-start(bf16[104,1024]{1,0:T(8,128)(2,1)S(1)} %collective-permute-done.1.below), channel_id=1, source_target_pairs={{0,96},{1,33},{2,98},{3,35},{4,100},{5,37},{6,102},{7,39},{8,104},... | collective-permute-start | bytes 638984 | tf_op jit(solution)/shard_map/ppermute | solution.py:335
  53.8 2.0 %collective-permute-start.3 = (bf16[96,1024]{1,0:T(8,128)(2,1)S(1)}, bf16[96,1024]{1,0:T(8,128)(2,1)S(1)}, u32[]{:S(2)}, u32[]{:S(2)}) collective-permute-start(bf16[96,1024]{1,0:T(8,128)(2,1)S(1)} %get-tuple-element.31), channel_id=1, source_target_pairs={{0,1},{1,0},{2,3},{3,2},{4,5},{5,4},{6,7},{7,6},{8,9},{9,8},{10,11... | collective-permute-start | bytes 589832 | tf_op jit(solution)/shard_map/ppermute | solution.py:340
  107.6 1.2 copy-start
  107.6 1.5 copy-start.1
  107.7 5.6 %collective-permute-start.5 = (bf16[512,1024]{1,0:T(8,128)(2,1)S(1)}, bf16[512,1024]{1,0:T(8,128)(2,1)S(1)}, u32[]{:S(2)}, u32[]{:S(2)}) collective-permute-start(bf16[512,1024]{1,0:T(8,128)(2,1)S(1)} %slice.8), channel_id=1, source_target_pairs={{0,1},{1,0},{2,3},{3,2},{4,5},{5,4},{6,7},{7,6},{8,9},{9,8},{10,11... | collective-permute-start | bytes 3145736 | tf_op jit(solution)/shard_map/ppermute | solution.py:340
  107.9 3.7 %collective-permute-start.7 = (bf16[384,1024]{1,0:T(8,128)(2,1)S(1)}, bf16[384,1024]{1,0:T(8,128)(2,1)S(1)}, u32[]{:S(2)}, u32[]{:S(2)}) collective-permute-start(bf16[384,1024]{1,0:T(8,128)(2,1)S(1)} %slice.9), channel_id=1, source_target_pairs={{0,1},{1,0},{2,3},{3,2},{4,5},{5,4},{6,7},{7,6},{8,9},{9,8},{10,11... | collective-permute-start | bytes 2359304 | tf_op jit(solution)/shard_map/ppermute | solution.py:340
  109.1 2.4 %copy-start.4 = (bf16[1,256,2048]{2,1,0:T(8,128)(2,1)S(1)}, bf16[1,256,2048]{2,1,0:T(8,128)(2,1)}, u32[]{:S(2)}) copy-start(bf16[1,256,2048]{2,1,0:T(8,128)(2,1)} %param.34) | copy-start | bytes 3145732
  112.8 2.6 %collective-permute-start.8 = (bf16[384,1024]{1,0:T(8,128)(2,1)S(1)}, bf16[384,1024]{1,0:T(8,128)(2,1)S(1)}, u32[]{:S(2)}, u32[]{:S(2)}) collective-permute-start(bf16[384,1024]{1,0:T(8,128)(2,1)S(1)} %get-tuple-element.40), channel_id=1, source_target_pairs={{0,1},{1,0},{2,3},{3,2},{4,5},{5,4},{6,7},{7,6},{8,9},{9,8},{10,11... | collective-permute-start | bytes 2359304 | tf_op jit(solution)/shard_map/ppermute | solution.py:340
  114.7 2.8 %collective-permute-start.6 = (bf16[512,1024]{1,0:T(8,128)(2,1)S(1)}, bf16[512,1024]{1,0:T(8,128)(2,1)S(1)}, u32[]{:S(2)}, u32[]{:S(2)}) collective-permute-start(bf16[512,1024]{1,0:T(8,128)(2,1)S(1)} %get-tuple-element.38), channel_id=1, source_target_pairs={{0,1},{1,0},{2,3},{3,2},{4,5},{5,4},{6,7},{7,6},{8,9},{9,8},{10,11... | collective-permute-start | bytes 3145736 | tf_op jit(solution)/shard_map/ppermute | solution.py:340
  157.3 20.4 %collective-permute-start.10 = (bf16[96,1024]{1,0:T(8,128)(2,1)S(1)}, bf16[96,1024]{1,0:T(8,128)(2,1)S(1)}, u32[]{:S(2)}, u32[]{:S(2)}) collective-permute-start(bf16[96,1024]{1,0:T(8,128)(2,1)S(1)} %shard_map.212), channel_id=1, source_target_pairs={{0,32},{1,97},{2,34},{3,99},{4,36},{5,101},{6,38},{7,103},{8,40},{... | collective-permute-start | bytes 589832 | tf_op jit(solution)/shard_map/ppermute | solution.py:335
  158.6 21.4 %collective-permute-start.9 = (bf16[96,1024]{1,0:T(8,128)(2,1)S(1)}, bf16[96,1024]{1,0:T(8,128)(2,1)S(1)}, u32[]{:S(2)}, u32[]{:S(2)}) collective-permute-start(bf16[96,1024]{1,0:T(8,128)(2,1)S(1)} %get-tuple-element.42), channel_id=1, source_target_pairs={{0,32},{1,97},{2,34},{3,99},{4,36},{5,101},{6,38},{7,103},{8,40},{... | collective-permute-start | bytes 589832 | tf_op jit(solution)/shard_map/ppermute | solution.py:335
  177.8 10.9 %collective-permute-start.11 = (bf16[96,1024]{1,0:T(8,128)(2,1)S(1)}, bf16[96,1024]{1,0:T(8,128)(2,1)S(1)}, u32[]{:S(2)}, u32[]{:S(2)}) collective-permute-start(bf16[96,1024]{1,0:T(8,128)(2,1)S(1)} %add_convert_fusion.3), channel_id=1, source_target_pairs={{0,96},{1,33},{2,98},{3,35},{4,100},{5,37},{6,102},{7,39},{8,104},... | collective-permute-start | bytes 589832 | tf_op jit(solution)/shard_map/ppermute | solution.py:335
